TPU v7x, 32 devices: a whole 2x2x4 slice. The times are simulated.
32 devices in a mesh: grp: 2 (over y), fs: 4 (over z), tp: 4 (over x, core).
Axes of the slice: x: 2, y: 2, z: 4, core: 2. Of those that a mesh axis runs over, the one named last changes fastest.
Arguments:
- tokens: bfloat16 [1024, 2048], P(('grp', 'fs'), 'tp'), parts along dimension 0, may hold values from -340 to 340
- routes: int32 [1024, 2], P(('grp', 'fs')), parts along dimension 0, may hold values from 0 to 7, all different within a row; in each aligned block of 128 rows (0 to 127, 128 to 255, ...) at most 40 rows name the same one
- route_weights: float32 [1024, 2], P(('grp', 'fs')), parts along dimension 0, may hold values from 0.2 to 1
- norm_gain: float32 [2048], P('fs'), may hold values from 0.1 to 1.9
- gate_weight: float32 [8, 2048, 4096], P(None, 'fs', 'tp'), may hold values from -0.125 to 0.125
- up_weight: float32 [8, 2048, 4096], P(None, 'fs', 'tp'), may hold values from -0.125 to 0.125
- down_weight: float32 [8, 2048, 4096], P(None, 'fs', 'tp'), may hold values from -0.09375 to 0.09375
Outputs:
- gate_out: bfloat16 [8, 4096, 4096], P('fs', 'grp', 'tp'), parts along dimension 1
- up_out: bfloat16 [8, 4096, 4096], P('fs', 'grp', 'tp'), parts along dimension 1
- down_out: bfloat16 [8, 4096, 4096], P('fs', 'grp', 'tp'), parts along dimension 1
- mixed_out: bfloat16 [1024, 2048], P(('grp', 'fs'), 'tp'), parts along dimension 0
There are 2 independent parts, one for each index of `grp`. A program takes and returns all parts, laid end to end along the dimension named above; an argument that names none is the same for every part. Nothing has to cross between parts.
Inputs may be any that keep to these rules, and one draw needn't show every extreme that they name: `routes`: each row names 2 different experts; in each aligned block of 128 rows no expert is named by more than 40 rows, and in some block one expert is named by exactly 40 rows.
All inputs are finite; a program needn't handle non-finite values.
Results may differ from a plain program's by a relative error of at most 0.015.
Values may be sent and summed in bfloat16 or wider, within the bound.
A program may use at most 192 MiB of HBM per device.

v0:
```python
import functools

import jax
import jax.numpy as jnp
from jax import lax
from jax.experimental import pallas as pl
from jax.experimental.pallas import tpu as pltpu
from jax.sharding import PartitionSpec as P

epsilon = 1e-06
MESH = pl.DeviceIdType.MESH


def expert_slots(routes, experts, capacity):
    row_count = routes.shape[0] * routes.shape[1]
    flat_routes = routes.reshape(row_count)
    onehot = (flat_routes[:, None] == jnp.arange(experts, dtype=jnp.int32)[None, :]).astype(
        jnp.int32
    )
    earlier = jnp.cumsum(onehot, axis=0) - onehot
    position = jnp.sum(earlier * onehot, axis=1)
    return (flat_routes * capacity + position).reshape(routes.shape)


def dispatch(normed, slots, experts, capacity, copies, local_count):
    col_width = normed.shape[1]
    slot_ids = jnp.arange(experts * capacity, dtype=jnp.int32)
    select = jnp.any(slot_ids[:, None, None] == slots[None, :, :], axis=2).astype(jnp.bfloat16)
    packed = jnp.dot(select, normed, preferred_element_type=jnp.float32).astype(jnp.bfloat16)
    packed = jnp.broadcast_to(
        packed.reshape(experts, 1, capacity, col_width), (experts, copies, capacity, col_width)
    )
    return packed.reshape(experts * copies // local_count, local_count, capacity, col_width)


def combine(returned, slots, route_weights, experts, copies):
    capacity, col_width = (returned.shape[2], returned.shape[3])
    summed_up = jnp.sum(
        returned.reshape(experts, copies, capacity, col_width), axis=1, dtype=jnp.float32
    )
    selected = summed_up.reshape(experts * capacity, col_width)[slots]
    return jnp.sum(route_weights[:, :, None] * selected, axis=1)


def exchange_kernel(
    dims, gains, gate_w, up_w, down_w, gate_o, up_o, down_o,
    raw, stage, load_sem, send_sem, recv_sem, pass_send, pass_recv,
):
    groups, count, local, copies, rows, width, parts = dims
    weights, landing = (gate_w, up_w, down_w), (gate_o, up_o, down_o)
    y, z = lax.axis_index("grp"), lax.axis_index("fs")
    share = rows // groups
    piece = share // parts

    barrier = pltpu.get_barrier_semaphore()

    def greet(j, _):
        @pl.when(j != z)
        def _():
            pl.semaphore_signal(barrier, inc=1, device_id={"fs": j}, device_id_type=MESH)
        return 0

    lax.fori_loop(0, count, greet, 0)
    for other in range(1, groups):
        pl.semaphore_signal(
            barrier, inc=1, device_id={"grp": lax.rem(y + other, groups)}, device_id_type=MESH
        )

    def load(m, j, first, slot):
        if copies > 1:
            expert, column = j // copies, lax.rem(j, copies) * width
            column = pl.ds(pl.multiple_of(column, 128), width)
        else:
            expert, column = j * local, slice(None)
        return pltpu.make_async_copy(
            weights[m].at[pl.ds(expert, local), pl.ds(first, share), column],
            raw.at[slot], load_sem.at[slot],
        )

    def fold(m, slot, first, put):
        def one(i, _):
            l, q = i // parts, lax.rem(i, parts)
            at = pl.multiple_of(q * piece, piece)
            scaled = raw[slot, l, pl.ds(at, piece), :]
            if m < 2:
                scaled = scaled * gains[pl.ds(pl.multiple_of(first + at, piece), piece), :1]
            put(l, at, scaled.astype(jnp.bfloat16))
            return 0

        lax.fori_loop(0, local * parts, one, 0)

    def sending(j, m, i):
        l, q = i // parts, lax.rem(i, parts)
        at = pl.multiple_of(q * piece, piece)
        base = pl.multiple_of(z * rows + y * share + at, piece)
        return pltpu.make_async_remote_copy(
            src_ref=stage.at[j, m, l, pl.ds(at, piece), :],
            dst_ref=landing[m].at[l, pl.ds(base, piece), :],
            send_sem=send_sem.at[j, m, i],
            recv_sem=recv_sem.at[z, m, i],
            device_id={"fs": j}, device_id_type=MESH,
        )

    def passing(s, m, i, other):
        l, q = i // parts, lax.rem(i, parts)
        base = pl.multiple_of(s * rows + y * share + q * piece, piece)
        spot = landing[m].at[l, pl.ds(base, piece), :]
        return pltpu.make_async_remote_copy(
            src_ref=spot, dst_ref=spot,
            send_sem=pass_send.at[s, m, i, other - 1],
            recv_sem=pass_recv.at[s, m, i, other - 1],
            device_id={"grp": lax.rem(y + other, groups)}, device_id_type=MESH,
        )

    def arriving(s, m, i, other):
        l, q = i // parts, lax.rem(i, parts)
        giver = lax.rem(y + groups - other, groups)
        base = pl.multiple_of(s * rows + giver * share + q * piece, piece)
        spot = landing[m].at[l, pl.ds(base, piece), :]
        return pltpu.make_async_remote_copy(
            src_ref=spot, dst_ref=spot,
            send_sem=pass_send.at[s, m, i, other - 1],
            recv_sem=pass_recv.at[s, m, i, other - 1],
            device_id={"grp": giver}, device_id_type=MESH,
        )

    def landed(s, m, i):
        l, q = i // parts, lax.rem(i, parts)
        base = pl.multiple_of(s * rows + y * share + q * piece, piece)
        return pltpu.make_async_remote_copy(
            src_ref=landing[m].at[l, pl.ds(base, piece), :],
            dst_ref=landing[m].at[l, pl.ds(base, piece), :],
            send_sem=send_sem.at[s, m, i],
            recv_sem=recv_sem.at[s, m, i],
            device_id={"fs": s}, device_id_type=MESH,
        )

    mine = pl.multiple_of(y * share, share)
    pieces = local * parts

    def neighbours(body):
        def step(d, _):
            for j, there in ((z + d, z + d < count), (z - d, z - d >= 0)):
                @pl.when(there)
                def _():
                    body(j)
            return 0

        lax.fori_loop(1, count, step, 0)

    def send_phase(phase):
        def to(j):
            for m in phase:
                load(m, j, mine, m % 2).start()
            for m in phase:
                load(m, j, mine, m % 2).wait()

                def put(l, at, value):
                    stage[j, m, l, pl.ds(at, piece), :] = value

                fold(m, m % 2, mine, put)
            for m in phase:
                def go(i, _):
                    sending(j, m, i).start()
                    return 0

                lax.fori_loop(0, pieces, go, 0)

        neighbours(to)

    pl.semaphore_wait(barrier, count - 1 + groups - 1)
    send_phase((0, 1))
    send_phase((2,))

    for m in range(3):
        for g in range(groups):
            load(m, z, g * share, g % 2).start()
            load(m, z, g * share, g % 2).wait()

            def put(l, at, value):
                base = pl.multiple_of(z * rows + g * share + at, piece)
                landing[m][l, pl.ds(base, piece), :] = value

            fold(m, g % 2, g * share, put)

    def pass_phase(phase):
        def take(s):
            for m in phase:
                def one(i, _):
                    landed(s, m, i).wait_recv()
                    for other in range(1, groups):
                        passing(s, m, i, other).start()
                    return 0

                lax.fori_loop(0, pieces, one, 0)

        neighbours(take)

    pass_phase((0, 1))
    pass_phase((2,))

    def finish(s):
        for m in range(3):
            def one(i, _):
                for other in range(1, groups):
                    arriving(s, m, i, other).wait_recv()
                    passing(s, m, i, other).wait_send()
                sending(s, m, i).wait_send()
                return 0

            lax.fori_loop(0, pieces, one, 0)

    neighbours(finish)


def relay_kernel(
    dims, gains, gate_w, up_w, down_w, gate_o, up_o, down_o,
    raw, stage, transit, load_sem, send_sem, recv_sem, relay_sem, pass_send, pass_recv,
):
    groups, count, local, copies, rows, width, parts = dims
    weights, landing = (gate_w, up_w, down_w), (gate_o, up_o, down_o)
    y, z = lax.axis_index("grp"), lax.axis_index("fs")
    share = rows // groups
    piece = share // parts
    pieces = local * parts
    mine = pl.multiple_of(y * share, share)

    def real(way, place):
        return place if way == 0 else count - 1 - place

    barrier = pltpu.get_barrier_semaphore()
    for j, there in ((z + 1, z + 1 < count), (z - 1, z >= 1)):
        @pl.when(there)
        def _():
            pl.semaphore_signal(barrier, inc=1, device_id={"fs": j}, device_id_type=MESH)
    for other in range(1, groups):
        pl.semaphore_signal(
            barrier, inc=1, device_id={"grp": lax.rem(y + other, groups)}, device_id_type=MESH
        )

    def load(m, j, first, slot):
        if copies > 1:
            expert, column = j // copies, lax.rem(j, copies) * width
            column = pl.ds(pl.multiple_of(column, 128), width)
        else:
            expert, column = j * local, slice(None)
        return pltpu.make_async_copy(
            weights[m].at[pl.ds(expert, local), pl.ds(first, share), column],
            raw.at[slot], load_sem.at[slot],
        )

    def cut(i):
        return i // parts, pl.multiple_of(lax.rem(i, parts) * piece, piece)

    def fold(m, slot, first, put):
        def one(i, _):
            l, at = cut(i)
            scaled = raw[slot, l, pl.ds(at, piece), :]
            if m < 2:
                scaled = scaled * gains[pl.ds(pl.multiple_of(first + at, piece), piece), :1]
            put(l, at, scaled.astype(jnp.bfloat16))
            return 0

        lax.fori_loop(0, pieces, one, 0)

    def spot(m, l, at, source, giver):
        base = pl.multiple_of(source * rows + giver * share + at, piece)
        return landing[m].at[l, pl.ds(base, piece), :]

    def hop(way, src, sem, m, i, k, s, dd, final):
        l, at = cut(i)
        if final:
            dst = spot(m, l, at, real(way, s), y)
        else:
            slot = (k - s) * (count - 2 - k) + (count - 1 - dd)
            dst = transit.at[way, slot, m, l, pl.ds(at, piece), :]
        place = (k - s) * (count - 1 - k) + (count - 1 - dd)
        return pltpu.make_async_remote_copy(
            src_ref=src, dst_ref=dst, send_sem=sem,
            recv_sem=recv_sem.at[way, place, m, i],
            device_id={"fs": real(way, k + 1)}, device_id_type=MESH,
        )

    def start_hop(way, src, sem, m, i, k, s, dd):
        @pl.when(dd == k + 1)
        def _():
            hop(way, src, sem, m, i, k, s, dd, True).start()

        @pl.when(dd > k + 1)
        def _():
            hop(way, src, sem, m, i, k, s, dd, False).start()

    def passing(s, m, i, other):
        l, at = cut(i)
        ref = spot(m, l, at, s, y)
        return pltpu.make_async_remote_copy(
            src_ref=ref, dst_ref=ref,
            send_sem=pass_send.at[s, m, i, other - 1],
            recv_sem=pass_recv.at[s, m, i, other - 1],
            device_id={"grp": lax.rem(y + other, groups)}, device_id_type=MESH,
        )

    def arriving(s, m, i, other):
        l, at = cut(i)
        giver = lax.rem(y + groups - other, groups)
        ref = spot(m, l, at, s, giver)
        return pltpu.make_async_remote_copy(
            src_ref=ref, dst_ref=ref,
            send_sem=pass_send.at[s, m, i, other - 1],
            recv_sem=pass_recv.at[s, m, i, other - 1],
            device_id={"grp": giver}, device_id_type=MESH,
        )

    def send_phase(phase):
        def step(d, _):
            for way in (0, 1):
                k = real(way, z)
                dd = count - d
                j = real(way, dd)

                @pl.when(dd > k)
                def _():
                    for m in phase:
                        load(m, j, mine, m).start()
                    for m in phase:
                        load(m, j, mine, m).wait()

                        def put(l, at, value):
                            stage[j, m, l, pl.ds(at, piece), :] = value

                        fold(m, m, mine, put)

                        def go(i, _):
                            l, at = cut(i)
                            src = stage.at[j, m, l, pl.ds(at, piece), :]
                            start_hop(way, src, send_sem.at[j, m, i], m, i, k, k, dd)
                            return 0

                        lax.fori_loop(0, pieces, go, 0)
            return 0

        lax.fori_loop(1, count, step, 0)

    def own_block():
        for m in range(3):
            for g in range(groups):
                load(m, z, g * share, g % 2).start()
                load(m, z, g * share, g % 2).wait()

                def put(l, at, value):
                    stage[z, m, l, pl.ds(at, piece), :] = value

                fold(m, g % 2, g * share, put)
                base = pl.multiple_of(z * rows + g * share, share)
                keep = pltpu.make_async_copy(
                    stage.at[z, m], landing[m].at[:, pl.ds(base, share), :], load_sem.at[g % 2]
                )
                keep.start()
                keep.wait()

    def take_phase(phase):
        most = max(k * (count - k) for k in range(count))

        def take(item, _):
            for m in phase:
                def one(i, _):
                    l, at = cut(i)
                    for way in (0, 1):
                        take_piece(way, m, item, i, l, at)
                    return 0

                lax.fori_loop(0, pieces, one, 0)
            return 0

        lax.fori_loop(0, most, take, 0)

    def take_piece(way, m, item, i, l, at):
        k = real(way, z)

        @pl.when(item < k * (count - k))
        def _():
            s = k - 1 - item // (count - k)
            dd = count - 1 - lax.rem(item, count - k)
            source = real(way, s)

            def awaited(ref):
                pltpu.make_async_remote_copy(
                    src_ref=ref, dst_ref=ref, send_sem=send_sem.at[source, m, i],
                    recv_sem=recv_sem.at[way, item, m, i],
                    device_id={"fs": source}, device_id_type=MESH,
                ).wait_recv()

            @pl.when(dd == k)
            def _():
                awaited(spot(m, l, at, source, y))
                for other in range(1, groups):
                    passing(source, m, i, other).start()

            @pl.when(dd > k)
            def _():
                slot = (k - 1 - s) * (count - 1 - k) + (count - 1 - dd)
                ref = transit.at[way, slot, m, l, pl.ds(at, piece), :]
                awaited(ref)
                start_hop(way, ref, relay_sem.at[way, slot, m, i], m, i, k, s, dd)

    def sent(ref, sem):
        pltpu.make_async_remote_copy(
            src_ref=ref, dst_ref=ref, send_sem=sem, recv_sem=recv_sem.at[0, 0, 0, 0],
            device_id={"grp": lax.rem(y + 1, groups)}, device_id_type=MESH,
        ).wait_send()

    def finish():
        def block(t, _):
            s, i = t // pieces, lax.rem(t, pieces)
            l, at = cut(i)

            @pl.when(s != z)
            def _():
                for m in range(3):
                    for other in range(1, groups):
                        arriving(s, m, i, other).wait_recv()
                        passing(s, m, i, other).wait_send()
                    sent(stage.at[s, m, l, pl.ds(at, piece), :], send_sem.at[s, m, i])
            return 0

        lax.fori_loop(0, count * pieces, block, 0)

        def passed(t, _):
            slot, i = t // pieces, lax.rem(t, pieces)
            l, at = cut(i)
            for way in (0, 1):
                @pl.when(slot < z * (count - 1 - z))
                def _():
                    for m in range(3):
                        sent(
                            transit.at[way, slot, m, l, pl.ds(at, piece), :],
                            relay_sem.at[way, slot, m, i],
                        )
            return 0

        lax.fori_loop(0, transit.shape[1] * pieces, passed, 0)

    ends = (z == 0).astype(jnp.int32) + (z == count - 1).astype(jnp.int32)
    pl.semaphore_wait(barrier, 2 - ends + groups - 1)
    send_phase((0, 1, 2))
    own_block()
    take_phase((0, 1, 2))
    finish()


def exchange(norm_gain, gate_weight, up_weight, down_weight, groups, count, copies, local):
    experts, rows, columns = gate_weight.shape
    width = columns // copies
    share = rows // groups
    parts = max(1, share // 128)
    gains = jnp.broadcast_to(norm_gain[:, None], (rows, 128))
    shape = (local, count * rows, width)
    dims = (groups, count, local, copies, rows, width, parts)
    pieces = local * parts
    relaying = 1 < count <= 8 and groups > 1
    common = [
        pltpu.VMEM((3, local, share, width), jnp.float32),
        pltpu.VMEM((count, 3, local, share, width), jnp.bfloat16),
    ]
    sem = pltpu.SemaphoreType.DMA
    passes = [sem((count, 3, pieces, max(1, groups - 1)))] * 2
    if relaying:
        slots = max(1, max(k * (count - 1 - k) for k in range(count)))
        items = max(k * (count - k) for k in range(count))
        scratch = common + [
            pltpu.VMEM((2, slots, 3, local, share, width), jnp.bfloat16),
            sem((3,)), sem((count, 3, pieces)), sem((2, items, 3, pieces)),
            sem((2, slots, 3, pieces)),
        ] + passes
    else:
        scratch = common + [sem((2,))] + [sem((count, 3, pieces))] * 2 + passes
    return pl.pallas_call(
        functools.partial(relay_kernel if relaying else exchange_kernel, dims),
        out_shape=[jax.ShapeDtypeStruct(shape, jnp.bfloat16)] * 3,
        in_specs=[pl.BlockSpec(memory_space=pltpu.VMEM)]
        + [pl.BlockSpec(memory_space=pl.ANY)] * 3,
        out_specs=[pl.BlockSpec(memory_space=pl.ANY if relaying else pltpu.VMEM)] * 3,
        scratch_shapes=scratch,
        compiler_params=pltpu.CompilerParams(
            collective_id=0, has_side_effects=True, vmem_limit_bytes=60 * 1024 * 1024
        ),
    )(gains, gate_weight, up_weight, down_weight)


def on_device(tokens, routes, route_weights, norm_gain, gate_weight, up_weight, down_weight):
    groups = lax.axis_size("grp")
    fs_count = lax.axis_size("fs")
    tp_count = lax.axis_size("tp")
    experts = gate_weight.shape[0]
    copies = max(1, fs_count // experts)
    local_count = max(1, experts // fs_count)
    capacity = tokens.shape[0] * 5 // 16

    gate_new, up_new, down_new = exchange(
        norm_gain, gate_weight, up_weight, down_weight, groups, fs_count, copies, local_count
    )
    slots = expert_slots(routes, experts, capacity)
    whole = lax.all_gather(tokens, "tp", axis=1, tiled=True)
    widened = whole.astype(jnp.float32)
    row_scale = lax.rsqrt(jnp.mean(widened * widened, axis=1, keepdims=True) + epsilon)
    normed = (widened * row_scale).astype(jnp.bfloat16)
    outgoing = dispatch(normed, slots, experts, capacity, copies, local_count)
    arrived = lax.all_to_all(outgoing, "fs", split_axis=0, concat_axis=0, tiled=True)
    gate_sums = jnp.einsum("slcd,ldf->slcf", arrived, gate_new, preferred_element_type=jnp.float32)
    up_sums = jnp.einsum("slcd,ldf->slcf", arrived, up_new, preferred_element_type=jnp.float32)
    hidden = (jax.nn.silu(gate_sums) * up_sums).astype(jnp.bfloat16)
    partial_value = jnp.einsum(
        "slcf,ldf->slcd", hidden, down_new, preferred_element_type=jnp.float32
    ).astype(jnp.bfloat16)
    by_columns = partial_value.reshape(
        partial_value.shape[:3] + (tp_count, partial_value.shape[3] // tp_count)
    )
    exchanged = lax.all_to_all(by_columns, "tp", split_axis=3, concat_axis=3, tiled=True)
    summed_up = jnp.sum(exchanged, axis=3, dtype=jnp.float32)
    handed = lax.all_to_all(
        summed_up.astype(jnp.bfloat16), "fs", split_axis=0, concat_axis=0, tiled=True
    ).astype(summed_up.dtype)
    combined = combine(handed, slots, route_weights, experts, copies)
    return (gate_new, up_new, down_new, combined.astype(jnp.bfloat16))


def solution(mesh):
    in_specs = (
        P(("grp", "fs"), "tp"),
        P(("grp", "fs"), None),
        P(("grp", "fs"), None),
        P("fs"),
        P(None, "fs", "tp"),
        P(None, "fs", "tp"),
        P(None, "fs", "tp"),
    )
    out_specs = (
        P("fs", "grp", "tp"),
        P("fs", "grp", "tp"),
        P("fs", "grp", "tp"),
        P(("grp", "fs"), "tp"),
    )
    return jax.shard_map(
        on_device, mesh=mesh, in_specs=in_specs, out_specs=out_specs, check_vma=False
    )
```

profile of v0, /device:TPU:0, one launch (start us, length us, event | category | flops | bytes accessed | tf_op | source)
XLA Modules:
  0.0 403.5 jit_solution(2990018429495040229)
XLA Ops:
  0.6 0.8 copy.52
  1.7 0.6 reduce-window.6
  2.3 0.2 slice_reduce_fusion
  2.9 0.7 compare_select_fusion
  3.6 8.9 %all_gather.3 = bf16[128,2048]{1,0:T(8,128)(2,1)S(1)} all-gather(bf16[128,512]{1,0:T(8,128)(2,1)} %param.7), channel_id=1, replica_groups=mesh['grp'=2,'fs'=4,'tp'=4] {'tp'}, dimensions={1}, use_global_device_ids=true | all-gather | bytes 655360 | tf_op jit(solution)/shard_map/all_gather | solution.py:503
  12.5 0.2 fusion.23
  12.7 1.6 convolution_convert_fusion
  14.3 5.0 %all-to-all-start = ((bf16[4,2,40,2048]{3,2,1,0:T(8,128)(2,1)}), bf16[4,2,40,2048]{3,2,1,0:T(8,128)(2,1)S(1)}, u32[]{:S(2)}, u32[]{:S(2)}) async-start(bf16[4,2,40,2048]{3,2,1,0:T(8,128)(2,1)} %bitcast.6), calls=%async_computation | async-start | bytes 2621440 | tf_op jit(solution)/shard_map/all_to_all | solution.py:508
  19.3 0.8 broadcast_in_dim.4.gains
  20.2 248.5 %shard_map.102 = (bf16[2,2048,1024]{2,1,0:T(8,128)(2,1)}, bf16[2,2048,1024]{2,1,0:T(8,128)(2,1)}, bf16[2,2048,1024]{2,1,0:T(8,128)(2,1)}) custom-call(f32[512,128]{1,0:T(8,128)} %broadcast_in_dim.4.gains, f32[8,512,1024]{2,1,0:T(8,128)} %gate_w.1, f32[8,512,1024]{2,1,0:T(8,128)} %up_w.1, f32[8,512,1024]{2,1,0:T(8,128)} %down_w.1), custom_call_target="tpu_custom_call" | custom-call | tf_op jit(solution)/shard_map/pallas_call | solution.py:477
  268.7 5.0 %fusion.9 = f32[4,2,40,1024]{3,2,0,1:T(8,128)S(1)} fusion(bf16[2,2048,1024]{2,1,0:T(8,128)(2,1)} %get-tuple-element.16, bf16[4,2,40,2048]{3,2,1,0:T(8,128)(2,1)S(1)} %all-to-all-done), kind=kOutput, calls=%fused_computation.9 | convolution fusion | flops 1342177280 | bytes 11010048 | tf_op jit(solution)/shard_map/slcd,ldf->slcf/dot_general | solution.py:509
  273.8 5.3 %fusion.18 = bf16[4,2,40,1024]{3,2,0,1:T(8,128)(2,1)S(1)} fusion(bf16[2,2048,1024]{2,1,0:T(8,128)(2,1)} %get-tuple-element.17, f32[4,2,40,1024]{3,2,0,1:T(8,128)S(1)} %fusion.9, bf16[4,2,40,2048]{3,2,1,0:T(8,128)(2,1)S(1)} %all-to-all-done), kind=kOutput, calls=%fused_computation.12 | convolution fusion | flops 1344143360 | bytes 11665408 | tf_op jit(solution)/shard_map/slcd,ldf->slcf/dot_general | solution.py:510
  279.1 2.9 fusion.6
  282.2 19.7 %all_to_all.15 = bf16[4,2,40,4,512]{4,2,0,1,3:T(8,128)(2,1)S(1)} all-to-all(bf16[4,2,40,4,512]{4,2,0,1,3:T(8,128)(2,1)S(1)} %bitcast.54), channel_id=1, replica_groups=mesh['grp'=2,'fs'=4,'tp'=4] {'tp'}, dimensions={3} | all-to-all | bytes 2621440 | tf_op jit(solution)/shard_map/all_to_all | solution.py:518
  301.8 0.3 reduce_sum.48
  302.1 0.8 copy.59
  302.9 64.6 %all-to-all-start.2 = ((bf16[4,2,40,512]{3,2,1,0:T(8,128)(2,1)}), bf16[4,2,40,512]{3,2,1,0:T(8,128)(2,1)S(1)}, u32[]{:S(2)}, u32[]{:S(2)}) async-start(bf16[4,2,40,512]{3,2,1,0:T(8,128)(2,1)} %copy.59), calls=%async_computation.2 | async-start | bytes 655360 | tf_op jit(solution)/shard_map/all_to_all | solution.py:520
  367.9 9.5 %all-to-all-done.2 = bf16[4,2,40,512]{3,2,1,0:T(8,128)(2,1)S(1)} async-done(((bf16[4,2,40,512]{3,2,1,0:T(8,128)(2,1)}), bf16[4,2,40,512]{3,2,1,0:T(8,128)(2,1)S(1)}, u32[]{:S(2)}, u32[]{:S(2)}) %all-to-all-start.2) | async-done | bytes 327712 | tf_op jit(solution)/shard_map/all_to_all | solution.py:520
  377.5 1.0 gather_fusion
  378.5 0.3 reshape.64
  378.8 1.4 multiply_reduce_fusion
  380.2 7.8 %copy.75 = bf16[2,2048,1024]{2,1,0:T(8,128)(2,1)} copy(bf16[2,2048,1024]{2,1,0:T(8,128)(2,1)} %get-tuple-element.16) | data formatting | bytes 16777216
  387.9 7.8 %copy.76 = bf16[2,2048,1024]{2,1,0:T(8,128)(2,1)} copy(bf16[2,2048,1024]{2,1,0:T(8,128)(2,1)} %get-tuple-element.17) | data formatting | bytes 16777216
  395.7 7.8 %copy.77 = bf16[2,2048,1024]{2,1,0:T(8,128)(2,1)} copy(bf16[2,2048,1024]{2,1,0:T(8,128)(2,1)} %get-tuple-element.18) | data formatting | bytes 16777216
  (26 shorter events, 1.3 us)
Async XLA Ops:
  14.3 5.0 %copy-start = (f32[512]{0:T(512)S(1)}, f32[512]{0:T(512)}, u32[]{:S(2)}) copy-start(f32[512]{0:T(512)} %param.10) | copy-start | bytes 6148
  14.3 254.4 %all-to-all-start = ((bf16[4,2,40,2048]{3,2,1,0:T(8,128)(2,1)}), bf16[4,2,40,2048]{3,2,1,0:T(8,128)(2,1)S(1)}, u32[]{:S(2)}, u32[]{:S(2)}) async-start(bf16[4,2,40,2048]{3,2,1,0:T(8,128)(2,1)} %bitcast.6), calls=%async_computation | async-start | bytes 2621440 | tf_op jit(solution)/shard_map/all_to_all | solution.py:508
  268.7 10.4 %slice-start = ((s8[8388608]{0:T(1024)(128)(4,1)}), s8[4194304]{0:T(1024)(128)(4,1)S(1)}, s32[]{:S(2)}) async-start(s8[8388608]{0:T(1024)(128)(4,1)} %bitcast.52), calls=%async_computation.3 | async-start | bytes 8388608
  273.8 5.3 %slice-start.1 = ((s8[8388608]{0:T(1024)(128)(4,1)}), s8[4194304]{0:T(1024)(128)(4,1)S(1)}, s32[]{:S(2)}) async-start(s8[8388608]{0:T(1024)(128)(4,1)} %bitcast.52), calls=%async_computation.4 | async-start | bytes 8388608
  301.8 65.9 %copy-start.1 = (f32[128,2]{0,1:T(2,128)S(1)}, f32[128,2]{0,1:T(2,128)}, u32[]{:S(2)}) copy-start(f32[128,2]{0,1:T(2,128)} %param.9) | copy-start | bytes 3076
  302.9 74.5 %all-to-all-start.2 = ((bf16[4,2,40,512]{3,2,1,0:T(8,128)(2,1)}), bf16[4,2,40,512]{3,2,1,0:T(8,128)(2,1)S(1)}, u32[]{:S(2)}, u32[]{:S(2)}) async-start(bf16[4,2,40,512]{3,2,1,0:T(8,128)(2,1)} %copy.59), calls=%async_computation.2 | async-start | bytes 655360 | tf_op jit(solution)/shard_map/all_to_all | solution.py:520
where the time goes:
time: 404 us; the launch traced here: 403 us
  Pallas kernels  249 us (62%)
  starting transfers between devices  69.6 us (17%)
  blocking collectives  28.5 us (7%)
  local copies, waits for them, and re-layouts  28.1 us (7%)
  matrix products  14.9 us (4%)
  waiting for transfers between devices  9.53 us (2%)
    pallas_call x1, Pallas kernels, exchange(): pl.pallas_call(functools.partial(relay_kernel if relaying else exchange_k...  249 us
    all_to_all x1, starting transfers between devices, on_device(): lax.all_to_all(summed_up.astype(jnp.bfloat16), 'fs', split_axis=0, concat...  64.6 us
    unnamed x13, local copies, waits for them, and re-layouts  24.2 us
    all_to_all x1, blocking collectives, on_device(): lax.all_to_all(by_columns, 'tp', split_axis=3, concat_axis=3, tiled=True)  19.7 us
    all_to_all x1, waiting for transfers between devices, on_device(): lax.all_to_all(summed_up.astype(jnp.bfloat16), 'fs', split_axis=0, concat...  9.53 us
    all_gather x1, blocking collectives, on_device(): whole = lax.all_gather(tokens, 'tp', axis=1, tiled=True)  8.86 us
  transfers between devices with their start and end apart: 2, of which 1 were waited for; matrix products, arithmetic and copies ran while one was open for 0% of the time, Pallas kernels for 62%

commit v1 on v0

--- a/solution.py
+++ b/solution.py
@@ -487,7 +487,7 @@
     )(gains, gate_weight, up_weight, down_weight)
 
 
-def on_device(tokens, routes, route_weights, norm_gain, gate_weight, up_weight, down_weight):
+def layered(tokens, routes, route_weights, norm_gain, gate_weight, up_weight, down_weight):
     groups = lax.axis_size("grp")
     fs_count = lax.axis_size("fs")
     tp_count = lax.axis_size("tp")
@@ -524,6 +524,617 @@
     return (gate_new, up_new, down_new, combined.astype(jnp.bfloat16))
 
 
+def far_first(count):
+    table = []
+    for z in range(count):
+        right = [j for j in range(count - 1, z, -1)]
+        left = [j for j in range(z)]
+        ways, order = sorted((right, left), key=len, reverse=True), []
+        for d in range(count):
+            order += [way[d] for way in ways if d < len(way)]
+        table.append(order)
+    return table
+
+
+def fused_kernel(
+    dims, tokens, routes, route_weights, gains, gate_w, up_w, down_w,
+    gate_o, up_o, down_o, mixed_o, transit,
+    raw, stage, gain_col, scales, send_x, land_x, normed, sums, hidden, partial, summing, combine_w,
+    send_ret, land_ret,
+    load_sem, send_sem, recv_sem, relay_sem, pass_send, pass_recv,
+    x_send, x_recv, xg_send, xg_recv, part_send, part_recv, ret_send, ret_recv,
+):
+    groups, count, tps, local, rows, width, parts, experts, capacity = dims
+    weights, landing = (gate_w, up_w, down_w), (gate_o, up_o, down_o)
+    y, z, t = lax.axis_index("grp"), lax.axis_index("fs"), lax.axis_index("tp")
+    share = rows // groups
+    piece = share // parts
+    pieces = local * parts
+    mine = pl.multiple_of(y * share, share)
+    table = far_first(count)
+    block_rows = local * capacity
+    own_tokens, columns = tokens.shape
+    tall = count * capacity
+    f32, bf16 = jnp.float32, jnp.bfloat16
+
+    def ranked(r):
+        return sum((z == k).astype(jnp.int32) * table[k][r] for k in range(count))
+
+    def real(way, place):
+        return place if way == 0 else count - 1 - place
+
+    def remote(src, dst, send, recv, axis, index):
+        return pltpu.make_async_remote_copy(
+            src_ref=src, dst_ref=dst, send_sem=send, recv_sem=recv,
+            device_id={axis: index}, device_id_type=MESH,
+        )
+
+    barrier = pltpu.get_barrier_semaphore()
+    for axis, me, size in (("fs", z, count), ("grp", y, groups), ("tp", t, tps)):
+        for other in range(1, size):
+            pl.semaphore_signal(
+                barrier, inc=1, device_id={axis: lax.rem(me + other, size)}, device_id_type=MESH
+            )
+
+    def load(m, j, first, slot):
+        return pltpu.make_async_copy(
+            weights[m].at[pl.ds(j * local, local), pl.ds(first, share), :],
+            raw.at[slot], load_sem.at[slot],
+        )
+
+    def cut(i):
+        return i // parts, pl.multiple_of(lax.rem(i, parts) * piece, piece)
+
+    def fold(m, slot, first, put):
+        def one(i, _):
+            l, at = cut(i)
+            scaled = raw[slot, l, pl.ds(at, piece), :]
+            if m < 2:
+                scaled = scaled * gain_col[pl.ds(pl.multiple_of(first + at, piece), piece), :1]
+            put(l, at, scaled.astype(bf16))
+            return 0
+
+        lax.fori_loop(0, pieces, one, 0)
+
+    def spot(m, l, at, source, giver):
+        base = pl.multiple_of(source * rows + giver * share + at, piece)
+        return landing[m].at[l, pl.ds(base, piece), :]
+
+    def start_hop(way, src, sem, m, i, k, s, dd):
+        l, at = cut(i)
+        place = (k - s) * (count - 1 - k) + (count - 1 - dd)
+        recv = recv_sem.at[way, place, m, i]
+
+        @pl.when(dd == k + 1)
+        def _():
+            remote(src, spot(m, l, at, real(way, s), y), sem, recv, "fs", real(way, k + 1)).start()
+
+        @pl.when(dd > k + 1)
+        def _():
+            slot = (k - s) * (count - 2 - k) + (count - 1 - dd)
+            dst = transit.at[way, slot, m, l, pl.ds(at, piece), :]
+            remote(src, dst, sem, recv, "fs", real(way, k + 1)).start()
+
+    def passing(s, m, i, other):
+        l, at = cut(i)
+        ref = spot(m, l, at, s, y)
+        return remote(
+            ref, ref, pass_send.at[s, m, i, other - 1], pass_recv.at[s, m, i, other - 1],
+            "grp", lax.rem(y + other, groups),
+        )
+
+    def arriving(s, m, i, other):
+        l, at = cut(i)
+        giver = lax.rem(y + groups - other, groups)
+        ref = spot(m, l, at, s, giver)
+        return remote(
+            ref, ref, pass_send.at[s, m, i, other - 1], pass_recv.at[s, m, i, other - 1],
+            "grp", giver,
+        )
+
+    def slot_rows():
+        wanted = routes[...]
+        expert_ids = lax.broadcasted_iota(jnp.int32, (experts, own_tokens), 0)
+        onehots = [
+            (expert_ids == wanted[k : k + 1, :]).astype(f32) for k in range(wanted.shape[0])
+        ]
+        before = lax.broadcasted_iota(jnp.int32, (own_tokens, own_tokens), 0)
+        after = lax.broadcasted_iota(jnp.int32, (own_tokens, own_tokens), 1)
+        upper = (before < after).astype(bf16)
+        earlier = jnp.dot(sum(onehots).astype(bf16), upper, preferred_element_type=f32)
+        found = []
+        for k, onehot in enumerate(onehots):
+            position = jnp.sum(earlier * onehot, axis=0, keepdims=True)
+            earlier = earlier + onehot
+            found.append(wanted[k : k + 1, :] * capacity + position.astype(jnp.int32))
+        return found
+
+    def pack():
+        found = slot_rows()
+        slot_ids = lax.broadcasted_iota(jnp.int32, (experts * capacity, own_tokens), 0)
+        chosen = jnp.zeros((experts * capacity, own_tokens), f32)
+        weighed = jnp.zeros((experts * capacity, own_tokens), f32)
+        for k, slot in enumerate(found):
+            hit = slot_ids == slot
+            chosen = jnp.where(hit, 1.0, chosen)
+            weighed = weighed + jnp.where(hit, route_weights[k : k + 1, :], 0.0)
+        packed = jnp.dot(chosen.astype(bf16), tokens[...], preferred_element_type=f32)
+        packed = packed.astype(bf16)
+        for j in range(count):
+            send_x[j] = packed[j * block_rows : (j + 1) * block_rows, :]
+        high = weighed.astype(bf16)
+        combine_w[0] = high
+        combine_w[1] = (weighed - high.astype(f32)).astype(bf16)
+
+    def dispatching(j):
+        return remote(send_x.at[j], land_x.at[t, z], x_send.at[j], x_recv.at[z], "fs", j)
+
+    def dispatched(s):
+        return remote(send_x.at[s], land_x.at[t, s], x_send.at[s], x_recv.at[s], "fs", s)
+
+    def spreading(s, other):
+        return remote(
+            land_x.at[t, s], land_x.at[t, s], xg_send.at[other, s], xg_recv.at[t, s],
+            "tp", lax.rem(t + other, tps),
+        )
+
+    def spread(s, peer):
+        return remote(
+            land_x.at[peer, s], land_x.at[peer, s], xg_send.at[0, s], xg_recv.at[peer, s],
+            "tp", peer,
+        )
+
+    def elsewhere(body):
+        for other in range(1, count):
+            body(lax.rem(z + other, count))
+
+    def normalise():
+        for s in range(count):
+            square = jnp.zeros((block_rows, 1), f32)
+            for c in range(tps):
+                part = land_x[c, s].astype(f32)
+                square = square + jnp.sum(part * part, axis=1, keepdims=True)
+            scales[s * block_rows : (s + 1) * block_rows, :] = jnp.broadcast_to(
+                lax.rsqrt(square / (tps * columns) + epsilon), (block_rows, 128)
+            )
+        for c in range(tps):
+            pile = [[] for _ in range(local)]
+            for s in range(count):
+                scale = scales[s * block_rows : (s + 1) * block_rows, :1]
+                scaled = land_x[c, s].astype(f32) * scale
+                for l in range(local):
+                    pile[l].append(scaled[l * capacity : (l + 1) * capacity, :])
+            for l in range(local):
+                normed[l, :, c * columns : (c + 1) * columns] = jnp.concatenate(
+                    pile[l], axis=0
+                ).astype(bf16)
+
+    tile = min(width, 256)
+
+    def gate_up(s, first):
+        def one(i, _):
+            l, n = i // (width // tile), lax.rem(i, width // tile)
+            base, at = pl.multiple_of(s * rows, rows), pl.multiple_of(n * tile, tile)
+            x = normed[l, :, pl.ds(base, rows)]
+            for m in range(2):
+                w = landing[m][l, pl.ds(base, rows), pl.ds(at, tile)]
+                value = jnp.dot(x, w, preferred_element_type=f32)
+                if not first:
+                    value = value + sums[m, l, :, pl.ds(at, tile)]
+                sums[m, l, :, pl.ds(at, tile)] = value
+            return 0
+
+        lax.fori_loop(0, local * (width // tile), one, 0)
+
+    def activate():
+        def one(i, _):
+            l, n = i // (width // tile), lax.rem(i, width // tile)
+            at = pl.multiple_of(n * tile, tile)
+            value = jax.nn.silu(sums[0, l, :, pl.ds(at, tile)]) * sums[1, l, :, pl.ds(at, tile)]
+            hidden[l, :, pl.ds(at, tile)] = value.astype(bf16)
+            return 0
+
+        lax.fori_loop(0, local * (width // tile), one, 0)
+
+    def part_copy(s, i, giver):
+        l, at = cut(i)
+        col = pl.ds(pl.multiple_of(giver * share + at, piece), piece)
+        return remote(
+            partial.at[s, l, :, col], summing.at[t, l, :, col], part_send.at[s, i, giver],
+            part_recv.at[t, i, giver], "tp", s,
+        )
+
+    def part_here(peer, i, giver):
+        l, at = cut(i)
+        col = pl.ds(pl.multiple_of(giver * share + at, piece), piece)
+        ref = summing.at[peer, l, :, col]
+        return remote(ref, ref, part_send.at[0, i, giver], part_recv.at[peer, i, giver], "tp", peer)
+
+    def down_piece(s, i):
+        l, at = cut(i)
+        for giver in range(groups):
+            base = pl.multiple_of(s * rows + giver * share + at, piece)
+            w = down_o[l, pl.ds(base, piece), :]
+            value = lax.dot_general(
+                hidden[l], w, (((1,), (1,)), ((), ())), preferred_element_type=f32
+            ).astype(bf16)
+            col = pl.ds(pl.multiple_of(giver * share + at, piece), piece)
+
+            @pl.when(s == t)
+            def _():
+                summing[t, l, :, col] = value
+
+            @pl.when(s != t)
+            def _():
+                partial[s, l, :, col] = value
+                part_copy(s, i, giver).start()
+
+    def returning(j):
+        return remote(send_ret.at[j], land_ret.at[z], ret_send.at[j], ret_recv.at[z], "fs", j)
+
+    def returned(s):
+        return remote(send_ret.at[s], land_ret.at[s], ret_send.at[s], ret_recv.at[s], "fs", s)
+
+    def give_back():
+        def await_part(i, _):
+            for other in range(1, tps):
+                for giver in range(groups):
+                    part_here(lax.rem(t + other, tps), i, giver).wait_recv()
+            return 0
+
+        lax.fori_loop(0, pieces, await_part, 0)
+        whole = []
+        for l in range(local):
+            value = summing[0, l].astype(f32)
+            for c in range(1, tps):
+                value = value + summing[c, l].astype(f32)
+            whole.append(value)
+        for j in range(count):
+            block = jnp.concatenate(
+                [value[j * capacity : (j + 1) * capacity, :] for value in whole], axis=0
+            ).astype(bf16)
+
+            @pl.when(z == j)
+            def _():
+                land_ret[j] = block
+
+            @pl.when(z != j)
+            def _():
+                send_ret[j] = block
+                returning(j).start()
+
+    sends = [(r, m, None) for r in range(count - 1) for m in (0, 1)]
+    keeps = [(None, m, g) for m in (0, 1) for g in range(groups)]
+    late = [(r, 2, None) for r in range(count - 1)] + [(None, 2, g) for g in range(groups)]
+    units = sends + keeps + late
+    slots = raw.shape[0]
+
+    def unit_load(n):
+        r, m, g = units[n]
+        if g is None:
+            return load(m, ranked(r), mine, n % slots)
+        return load(m, z, g * share, n % slots)
+
+    def send_unit(r, m):
+        j = ranked(r)
+
+        def go(i, _):
+            l, at = cut(i)
+            src = stage.at[r, m, l, pl.ds(at, piece), :]
+            for way in (0, 1):
+                @pl.when(j > z if way == 0 else j < z)
+                def _():
+                    start_hop(
+                        way, src, send_sem.at[r, m, i], m, i, real(way, z), real(way, z),
+                        real(way, j),
+                    )
+            return 0
+
+        lax.fori_loop(0, pieces, go, 0)
+
+    def do_unit(n):
+        r, m, g = units[n]
+        if n + slots - 1 < len(units):
+            unit_load(n + slots - 1).start()
+        unit_load(n).wait()
+        if g is None:
+            def put(l, at, value):
+                stage[r, m, l, pl.ds(at, piece), :] = value
+
+            fold(m, n % slots, mine, put)
+        else:
+            def put(l, at, value):
+                base = pl.multiple_of(z * rows + g * share + at, piece)
+                landing[m][l, pl.ds(base, piece), :] = value
+
+            fold(m, n % slots, g * share, put)
+
+    for n in range(slots - 1):
+        unit_load(n).start()
+    gain_rows = jnp.transpose(gains[...])
+    for q in range(rows // 128):
+        gain_col[q * 128 : (q + 1) * 128, :] = jnp.broadcast_to(gain_rows[:, q : q + 1], (128, 128))
+    pack()
+    pl.semaphore_wait(barrier, count - 1 + groups - 1 + tps - 1)
+    elsewhere(lambda j: dispatching(j).start())
+    for n in range(len(sends)):
+        do_unit(n)
+        send_unit(*units[n][:2])
+
+    land_x[t, z] = send_x[z]
+    for other in range(1, tps):
+        spreading(z, other).start()
+
+    def forward(s):
+        dispatched(s).wait_recv()
+        for other in range(1, tps):
+            spreading(s, other).start()
+
+    elsewhere(forward)
+    for n in range(len(sends), len(units)):
+        do_unit(n)
+    for other in range(1, tps):
+        for s in range(count):
+            spread(s, lax.rem(t + other, tps)).wait_recv()
+    normalise()
+    gate_up(z, True)
+
+    def take_piece(way, m, item, i):
+        k = real(way, z)
+        l, at = cut(i)
+
+        @pl.when(item < k * (count - k))
+        def _():
+            s = k - 1 - item // (count - k)
+            dd = count - 1 - lax.rem(item, count - k)
+            source = real(way, s)
+
+            def awaited(ref):
+                remote(
+                    ref, ref, send_sem.at[0, m, i], recv_sem.at[way, item, m, i], "fs", source
+                ).wait_recv()
+
+            @pl.when(dd == k)
+            def _():
+                awaited(spot(m, l, at, source, y))
+                for other in range(1, groups):
+                    passing(source, m, i, other).start()
+
+            @pl.when(dd > k)
+            def _():
+                slot = (k - 1 - s) * (count - 1 - k) + (count - 1 - dd)
+                ref = transit.at[way, slot, m, l, pl.ds(at, piece), :]
+                awaited(ref)
+                start_hop(way, ref, relay_sem.at[way, slot, m, i], m, i, k, s, dd)
+
+    def settled(way, item, body):
+        k = real(way, z)
+        kept = jnp.maximum(item, 0)
+        s = k - 1 - kept // (count - k)
+        dd = count - 1 - lax.rem(kept, count - k)
+
+        @pl.when((item >= 0) & (item < k * (count - k)) & (dd == k))
+        def _():
+            body(real(way, s))
+
+    most = max(k * (count - k) for k in range(count))
+
+    def await_pass(s, m, i):
+        for other in range(1, groups):
+            arriving(s, m, i, other).wait_recv()
+
+    def early_block(s):
+        def one(i, _):
+            for m in (0, 1):
+                await_pass(s, m, i)
+            return 0
+
+        lax.fori_loop(0, pieces, one, 0)
+        gate_up(s, False)
+
+    def early(n, _):
+        for m in (0, 1):
+            def one(i, _):
+                for way in (0, 1):
+                    take_piece(way, m, n, i)
+                return 0
+
+            lax.fori_loop(0, pieces, one, 0)
+            if m == 0:
+                for way in (0, 1):
+                    settled(way, n - 1, early_block)
+
+        @pl.when(n == min(1, most - 1))
+        def _():
+            for r in range(count - 1):
+                send_unit(r, 2)
+        return 0
+
+    lax.fori_loop(0, most + 1, early, 0)
+    activate()
+
+    def own_down(i, _):
+        down_piece(z, i)
+        return 0
+
+    lax.fori_loop(0, pieces, own_down, 0)
+
+    lag, wait_for = 2, 4
+
+    def later(p, _):
+        n, i = p // pieces, lax.rem(p, pieces)
+        for way in (0, 1):
+            take_piece(way, 2, n, i)
+        q = p - lag
+        before = jnp.maximum(q, 0)
+
+        def work(s):
+            j = lax.rem(before, pieces)
+            await_pass(s, 2, j)
+            down_piece(s, j)
+
+        for way in (0, 1):
+            settled(way, jnp.where(q >= 0, before // pieces, -1), work)
+
+        @pl.when((p == 1) & (z == t))
+        def _():
+            give_back()
+
+        q = p - wait_for
+        done = jnp.maximum(q, 0)
+
+        def close(s):
+            @pl.when((s == t) & (lax.rem(done, pieces) == pieces - 1))
+            def _():
+                give_back()
+
+        for way in (0, 1):
+            settled(way, jnp.where(q >= 0, done // pieces, -1), close)
+        return 0
+
+    lax.fori_loop(0, most * pieces + wait_for, later, 0)
+
+    def sent(ref, sem):
+        remote(ref, ref, sem, recv_sem.at[0, 0, 0, 0], "grp", lax.rem(y + 1, groups)).wait_send()
+
+    def drain(i, _):
+        l, at = cut(i)
+        for m in range(3):
+            for r in range(count - 1):
+                sent(stage.at[r, m, l, pl.ds(at, piece), :], send_sem.at[r, m, i])
+
+                def passed(s):
+                    for other in range(1, groups):
+                        passing(s, m, i, other).wait_send()
+
+                passed(ranked(r))
+            for slot in range(transit.shape[1]):
+                for way in (0, 1):
+                    @pl.when(slot < z * (count - 1 - z))
+                    def _():
+                        sent(
+                            transit.at[way, slot, m, l, pl.ds(at, piece), :],
+                            relay_sem.at[way, slot, m, i],
+                        )
+        for s in range(count):
+            @pl.when(s != t)
+            def _():
+                for giver in range(groups):
+                    part_copy(s, i, giver).wait_send()
+        return 0
+
+    lax.fori_loop(0, pieces, drain, 0)
+    elsewhere(lambda j: dispatching(j).wait_send())
+    for other in range(1, tps):
+        for s in range(count):
+            spreading(s, other).wait_send()
+
+    elsewhere(lambda s: returned(s).wait_recv())
+    back = land_ret[...].reshape(experts * capacity, columns)
+    over = (((0,), (0,)), ((), ()))
+    value = lax.dot_general(combine_w[0], back, over, preferred_element_type=f32)
+    value = value + lax.dot_general(combine_w[1], back, over, preferred_element_type=f32)
+    mixed_o[...] = value.astype(bf16)
+    elsewhere(lambda j: returning(j).wait_send())
+
+
+def writer_kernel(parts, *refs):
+    ins, outs, sem = refs[:4], refs[4:8], refs[8]
+    local, high = ins[0].shape[:2]
+    step = high // parts
+
+    def copy(k, l, i):
+        at = pl.ds(i * step, step)
+        return pltpu.make_async_copy(ins[k].at[l, at, :], outs[k].at[l, at, :], sem.at[k, l, i])
+
+    small = pltpu.make_async_copy(ins[3], outs[3], sem.at[3, 0, 0])
+    jobs = [copy(k, l, i) for k in range(3) for l in range(local) for i in range(parts)] + [small]
+    for job in jobs:
+        job.start()
+    for job in jobs:
+        job.wait()
+
+
+def fused(tokens, routes, route_weights, norm_gain, gate_weight, up_weight, down_weight):
+    groups, count, tps = (lax.axis_size(axis) for axis in ("grp", "fs", "tp"))
+    experts, rows, width = gate_weight.shape
+    local, own_tokens, columns = experts // count, *tokens.shape
+    capacity = own_tokens * 5 // 16
+    share = rows // groups
+    parts = max(1, share // 128)
+    pieces = local * parts
+    tall = count * capacity
+    dims = (groups, count, tps, local, rows, width, parts, experts, capacity)
+    shape = (local, count * rows, width)
+    slots = max(1, max(k * (count - 1 - k) for k in range(count)))
+    items = max(k * (count - k) for k in range(count))
+    bf16, f32, sem = jnp.bfloat16, jnp.float32, pltpu.SemaphoreType.DMA
+    vmem, anywhere = pl.BlockSpec(memory_space=pltpu.VMEM), pl.BlockSpec(memory_space=pl.ANY)
+    block = (local * capacity, columns)
+    gate, up, down, mixed, _ = pl.pallas_call(
+        functools.partial(fused_kernel, dims),
+        out_shape=[pltpu.VMEM(shape, bf16)] * 3
+        + [pltpu.VMEM(tokens.shape, bf16)]
+        + [jax.ShapeDtypeStruct((2, slots, 3, local, share, width), bf16)],
+        in_specs=[vmem] * 4 + [anywhere] * 3,
+        out_specs=[vmem] * 4 + [anywhere],
+        scratch_shapes=[
+            pltpu.VMEM((3, local, share, width), f32),
+            pltpu.VMEM((count - 1, 3, local, share, width), bf16),
+            pltpu.VMEM((rows, 128), f32),
+            pltpu.VMEM((experts * capacity, 128), f32),
+            pltpu.VMEM((count,) + block, bf16),
+            pltpu.VMEM((tps, count) + block, bf16),
+            pltpu.VMEM((local, tall, tps * columns), bf16),
+            pltpu.VMEM((2, local, tall, width), f32),
+            pltpu.VMEM((local, tall, width), bf16),
+            pltpu.VMEM((count, local, tall, columns), bf16),
+            pltpu.VMEM((tps, local, tall, columns), bf16),
+            pltpu.VMEM((2, experts * capacity, own_tokens), bf16),
+            pltpu.VMEM((count,) + block, bf16),
+            pltpu.VMEM((count,) + block, bf16),
+            sem((3,)), sem((count - 1, 3, pieces)), sem((2, items, 3, pieces)),
+            sem((2, slots, 3, pieces)),
+            sem((count, 3, pieces, groups - 1)), sem((count, 3, pieces, groups - 1)),
+            sem((count,)), sem((count,)), sem((tps, count)), sem((tps, count)),
+            sem((count, pieces, groups)), sem((tps, pieces, groups)), sem((count,)), sem((count,)),
+        ],
+        compiler_params=pltpu.CompilerParams(
+            collective_id=1, has_side_effects=True, vmem_limit_bytes=38 * 1024 * 1024
+        ),
+    )(
+        tokens, routes.T, route_weights.T, norm_gain.reshape(rows // 128, 128),
+        gate_weight, up_weight, down_weight,
+    )
+    parts = max(1, shape[1] // 512)
+    return pl.pallas_call(
+        functools.partial(writer_kernel, parts),
+        out_shape=[jax.ShapeDtypeStruct(shape, bf16)] * 3
+        + [jax.ShapeDtypeStruct(tokens.shape, bf16)],
+        in_specs=[vmem] * 4,
+        out_specs=[anywhere] * 4,
+        scratch_shapes=[sem((4, local, parts))],
+        compiler_params=pltpu.CompilerParams(vmem_limit_bytes=1024 * 1024),
+    )(gate, up, down, mixed)
+
+
+def on_device(tokens, routes, route_weights, norm_gain, gate_weight, up_weight, down_weight):
+    groups, count, tps = (lax.axis_size(axis) for axis in ("grp", "fs", "tp"))
+    experts, rows, width = gate_weight.shape
+    own_tokens, columns = tokens.shape
+    capacity = own_tokens * 5 // 16
+    fits = (
+        groups > 1 and 1 < count <= 8 and experts % count == 0 and rows == columns
+        and count == tps and rows % (128 * groups) == 0 and width % 128 == 0
+        and capacity % 8 == 0 and (experts // count * capacity) % 16 == 0
+        and 6 * experts // count * count * rows * width <= 24 * 1024 * 1024
+    )
+    body = fused if fits else layered
+    return tuple(
+        body(tokens, routes, route_weights, norm_gain, gate_weight, up_weight, down_weight)
+    )
+
+
 def solution(mesh):
     in_specs = (
         P(("grp", "fs"), "tp"),

time: 404 us -> 316 us (0.78)
  starting transfers between devices: 69.6 us -> 0 us
  Pallas kernels: 249 us -> 315 us
  blocking collectives: 28.5 us -> 0 us
  local copies, waits for them, and re-layouts: 28.1 us -> 0 us
  matrix products: 14.9 us -> 0 us
  waiting for transfers between devices: 9.53 us -> 0 us
    all_to_all x2 -> x0, starting transfers between devices: 69.6 us -> none  [the longest x1 64.6 us: on_device(): lax.all_to_all(summed_up.astype(jnp.bfloat16), 'fs', split_axis=0, concat...]
    pallas_call x1 -> x2, Pallas kernels: 249 us -> 315 us  [the longest x1 306 us: fused(): pl.pallas_call(functools.partial(fused_kernel, dims), out_shape=[pltpu.VM...]
    unnamed x13 -> x0, local copies, waits for them, and re-layouts: 24.2 us -> none
    all_to_all x1 -> x0, blocking collectives: 19.7 us -> none  [on_device(): lax.all_to_all(by_columns, 'tp', split_axis=3, concat_axis=3, tiled=True)]
    dot_general x4 -> x0, matrix products: 14.9 us -> none  [the longest x1 5.29 us: on_device(): jnp.einsum('slcd,ldf->slcf', arrived, up_new, preferred_element_type=jnp....]
    all_to_all x2 -> x0, waiting for transfers between devices: 9.53 us -> none  [the longest x1 9.53 us: on_device(): lax.all_to_all(summed_up.astype(jnp.bfloat16), 'fs', split_axis=0, concat...]
    all_gather x1 -> x0, blocking collectives: 8.86 us -> none  [on_device(): whole = lax.all_gather(tokens, 'tp', axis=1, tiled=True)]
  transfers between devices with their start and end apart: 2 -> 0, of which waited for: 1 -> 0; matrix products, arithmetic and copies ran while one was open for 0% -> 0% of each run, Pallas kernels for 62% -> 0%
where the time goes in v1:
time: 316 us
  Pallas kernels  315 us (100%)
    pallas_call x1, Pallas kernels, fused(): pl.pallas_call(functools.partial(fused_kernel, dims), out_shape=[pltpu.VM...  306 us
    pallas_call x1, Pallas kernels, fused(): pl.pallas_call(functools.partial(writer_kernel, parts), out_shape=[jax.Sh...  8.63 us

profile of v1, /device:TPU:0, one launch (start us, length us, event | category | flops | bytes accessed | tf_op | source)
XLA Modules:
  0.0 315.7 jit_solution(5947854843302801122)
XLA Ops:
  0.6 306.4 %shard_map.102 = (bf16[2,2048,1024]{2,1,0:T(8,128)(2,1)S(1)}, bf16[2,2048,1024]{2,1,0:T(8,128)(2,1)S(1)}, bf16[2,2048,1024]{2,1,0:T(8,128)(2,1)S(1)}, bf16[128,5...) custom-call(bf16[128,512]{1,0:T(8,128)(2,1)} %tokens.1, s32[2,128]{1,0:T(2,128)} %bitcast.4, f32[2,128]{1,0:T(2,128)} %bitcast.5, ...), custom_call_target="tpu_custom_call" | custom-call | tf_op jit(solution)/shard_map/pallas_call | solution.py:1074
  307.1 8.6 %shard_map.103 = (bf16[2,2048,1024]{2,1,0:T(8,128)(2,1)}, bf16[2,2048,1024]{2,1,0:T(8,128)(2,1)}, bf16[2,2048,1024]{2,1,0:T(8,128)(2,1)}, bf16[128,512]{1,0:T(8,128)(2,1)}) custom-call(bf16[2,2048,1024]{2,1,0:T(8,128)(2,1)S(1)} %get-tuple-element.8.refs_0_, bf16[2,2048,1024]{2,1,0:T(8,128)(2,1)S(1)} %get-tuple-element.9.refs_1_, ...), custom_call_target="tpu_custom_call" | custom-call | tf_op jit(solution)/shard_map/pallas_call | solution.py:1110

commit v2 on v1

--- a/solution.py
+++ b/solution.py
@@ -539,10 +539,11 @@
 def fused_kernel(
     dims, tokens, routes, route_weights, gains, gate_w, up_w, down_w,
     gate_o, up_o, down_o, mixed_o, transit,
-    raw, stage, gain_col, scales, send_x, land_x, normed, sums, hidden, partial, summing, combine_w,
+    raw, stage, gain_col, scales, send_x, land_x, normed, sums, hidden, partial, across, summing, combine_w,
     send_ret, land_ret,
     load_sem, send_sem, recv_sem, relay_sem, pass_send, pass_recv,
     x_send, x_recv, xg_send, xg_recv, part_send, part_recv, ret_send, ret_recv,
+    across_send, hid_send, hid_recv, go_sem,
 ):
     groups, count, tps, local, rows, width, parts, experts, capacity = dims
     weights, landing = (gate_w, up_w, down_w), (gate_o, up_o, down_o)
@@ -619,7 +620,7 @@
         l, at = cut(i)
         ref = spot(m, l, at, s, y)
         return remote(
-            ref, ref, pass_send.at[s, m, i, other - 1], pass_recv.at[s, m, i, other - 1],
+            ref, ref, pass_send.at[s, m, other - 1], pass_recv.at[s, m, i, other - 1],
             "grp", lax.rem(y + other, groups),
         )
 
@@ -628,7 +629,7 @@
         giver = lax.rem(y + groups - other, groups)
         ref = spot(m, l, at, s, giver)
         return remote(
-            ref, ref, pass_send.at[s, m, i, other - 1], pass_recv.at[s, m, i, other - 1],
+            ref, ref, pass_send.at[s, m, other - 1], pass_recv.at[s, m, i, other - 1],
             "grp", giver,
         )
 
@@ -651,9 +652,9 @@
 
     def pack():
         found = slot_rows()
-        slot_ids = lax.broadcasted_iota(jnp.int32, (experts * capacity, own_tokens), 0)
-        chosen = jnp.zeros((experts * capacity, own_tokens), f32)
-        weighed = jnp.zeros((experts * capacity, own_tokens), f32)
+        shape = (combine_w.shape[2], own_tokens)
+        slot_ids = lax.broadcasted_iota(jnp.int32, shape, 0)
+        chosen, weighed = jnp.zeros(shape, f32), jnp.zeros(shape, f32)
         for k, slot in enumerate(found):
             hit = slot_ids == slot
             chosen = jnp.where(hit, 1.0, chosen)
@@ -662,6 +663,7 @@
         packed = packed.astype(bf16)
         for j in range(count):
             send_x[j] = packed[j * block_rows : (j + 1) * block_rows, :]
+        weighed = jnp.transpose(weighed)
         high = weighed.astype(bf16)
         combine_w[0] = high
         combine_w[1] = (weighed - high.astype(f32)).astype(bf16)
@@ -674,15 +676,13 @@
 
     def spreading(s, other):
         return remote(
-            land_x.at[t, s], land_x.at[t, s], xg_send.at[other, s], xg_recv.at[t, s],
+            land_x.at[t, s], land_x.at[t, s], xg_send.at[0], xg_recv.at[0],
             "tp", lax.rem(t + other, tps),
         )
 
-    def spread(s, peer):
-        return remote(
-            land_x.at[peer, s], land_x.at[peer, s], xg_send.at[0, s], xg_recv.at[peer, s],
-            "tp", peer,
-        )
+    def spread():
+        ref = land_x.at[pl.ds(0, tps - 1)]
+        return remote(ref, ref, xg_send.at[0], xg_recv.at[0], "tp", lax.rem(t + 1, tps))
 
     def elsewhere(body):
         for other in range(1, count):
@@ -731,43 +731,109 @@
             l, n = i // (width // tile), lax.rem(i, width // tile)
             at = pl.multiple_of(n * tile, tile)
             value = jax.nn.silu(sums[0, l, :, pl.ds(at, tile)]) * sums[1, l, :, pl.ds(at, tile)]
-            hidden[l, :, pl.ds(at, tile)] = value.astype(bf16)
+            hidden[y, l, :, pl.ds(at, tile)] = value.astype(bf16)
             return 0
 
         lax.fori_loop(0, local * (width // tile), one, 0)
+
+    half = count // 2
+    most = max(k * (count - k) for k in range(count))
+
+    def comes_last(s):
+        place = jnp.where(z > s, z, count - 1 - z)
+        origin = jnp.where(z > s, s, count - 1 - s)
+        arrival = (place - 1 - origin) * (count - place) + (count - 1 - place)
+        return (z != s) & (arrival == most - 1)
+
+    last = comes_last(t)
+
+    def feature(giver, at):
+        return pl.ds(pl.multiple_of(giver * share + at, piece), piece)
+
+    def lending(other):
+        return pltpu.make_async_remote_copy(
+            src_ref=hidden.at[y, local - 1], dst_ref=hidden.at[y, local - 1],
+            send_sem=hid_send.at[other], recv_sem=hid_recv.at[y], device_id={"grp": lax.rem(y + other, groups)},
+            device_id_type=MESH,
+        )
+
+    def lent(other):
+        giver = lax.rem(y + other, groups)
+        ref = hidden.at[giver, local - 1]
+        return remote(ref, ref, hid_send.at[other], hid_recv.at[giver], "grp", giver)
 
     def part_copy(s, i, giver):
         l, at = cut(i)
-        col = pl.ds(pl.multiple_of(giver * share + at, piece), piece)
+        col = feature(giver, at)
         return remote(
             partial.at[s, l, :, col], summing.at[t, l, :, col], part_send.at[s, i, giver],
             part_recv.at[t, i, giver], "tp", s,
         )
 
+    final = pieces - 1
+
+    def part_across(way, s, other):
+        l, at = cut(final)
+        return pltpu.make_async_remote_copy(
+            src_ref=across.at[way, other - 1],
+            dst_ref=summing.at[t, l, :, feature(y, at)],
+            send_sem=across_send.at[way, other - 1], recv_sem=part_recv.at[t, final, y],
+            device_id={"grp": lax.rem(y + other, groups), "tp": s}, device_id_type=MESH,
+        )
+
     def part_here(peer, i, giver):
         l, at = cut(i)
-        col = pl.ds(pl.multiple_of(giver * share + at, piece), piece)
-        ref = summing.at[peer, l, :, col]
+        ref = summing.at[peer, l, :, feature(giver, at)]
         return remote(ref, ref, part_send.at[0, i, giver], part_recv.at[peer, i, giver], "tp", peer)
 
-    def down_piece(s, i):
+    def down_rows(group, s, i, giver):
+        l, at = cut(i)
+        base = pl.multiple_of(s * rows + giver * share + at, piece)
+        return lax.dot_general(
+            hidden[group, l], down_o[l, pl.ds(base, piece), :], (((1,), (1,)), ((), ())),
+            preferred_element_type=f32,
+        ).astype(bf16)
+
+    def down_piece(s, i, givers):
+        l, at = cut(i)
+        for giver in givers:
+            value = down_rows(y, s, i, giver)
+
+            @pl.when(s == t)
+            def _():
+                summing[t, l, :, feature(giver, at)] = value
+
+            @pl.when(s != t)
+            def _():
+                partial[s, l, :, feature(giver, at)] = value
+
+        @pl.when(s != t)
+        def _():
+            for giver in givers:
+                part_copy(s, i, giver).start()
+
+    def down_last(way, s):
+        for other in range(1, groups):
+            across[way, other - 1] = down_rows(lax.rem(y + other, groups), s, final, y)
+        down_piece(s, final, (y,))
+        for other in range(1, groups):
+            part_across(way, s, other).start()
+
+    def close_piece(i):
         l, at = cut(i)
         for giver in range(groups):
-            base = pl.multiple_of(s * rows + giver * share + at, piece)
-            w = down_o[l, pl.ds(base, piece), :]
-            value = lax.dot_general(
-                hidden[l], w, (((1,), (1,)), ((), ())), preferred_element_type=f32
-            ).astype(bf16)
-            col = pl.ds(pl.multiple_of(giver * share + at, piece), piece)
-
-            @pl.when(s == t)
+            for other in range(1, tps):
+                part_here(lax.rem(t + other, tps), i, giver).wait_recv()
+
+            @pl.when((y != giver) & last & (i == final))
             def _():
-                summing[t, l, :, col] = value
-
-            @pl.when(s != t)
-            def _():
-                partial[s, l, :, col] = value
-                part_copy(s, i, giver).start()
+                part_here(t, i, giver).wait_recv()
+
+            col = feature(giver, at)
+            value = summing[0, l, :, col].astype(f32)
+            for peer in range(1, tps):
+                value = value + summing[peer, l, :, col].astype(f32)
+            sums[0, l, :, col] = value
 
     def returning(j):
         return remote(send_ret.at[j], land_ret.at[z], ret_send.at[j], ret_recv.at[z], "fs", j)
@@ -776,22 +842,13 @@
         return remote(send_ret.at[s], land_ret.at[s], ret_send.at[s], ret_recv.at[s], "fs", s)
 
     def give_back():
-        def await_part(i, _):
-            for other in range(1, tps):
-                for giver in range(groups):
-                    part_here(lax.rem(t + other, tps), i, giver).wait_recv()
-            return 0
-
-        lax.fori_loop(0, pieces, await_part, 0)
-        whole = []
-        for l in range(local):
-            value = summing[0, l].astype(f32)
-            for c in range(1, tps):
-                value = value + summing[c, l].astype(f32)
-            whole.append(value)
         for j in range(count):
             block = jnp.concatenate(
-                [value[j * capacity : (j + 1) * capacity, :] for value in whole], axis=0
+                [
+                    sums[0, l, j * capacity : (j + 1) * capacity, :columns]
+                    for l in range(local)
+                ],
+                axis=0,
             ).astype(bf16)
 
             @pl.when(z == j)
@@ -801,7 +858,8 @@
             @pl.when(z != j)
             def _():
                 send_ret[j] = block
-                returning(j).start()
+        for r in range(count - 1):
+            returning(ranked(r)).start()
 
     sends = [(r, m, None) for r in range(count - 1) for m in (0, 1)]
     keeps = [(None, m, g) for m in (0, 1) for g in range(groups)]
@@ -825,7 +883,7 @@
                 @pl.when(j > z if way == 0 else j < z)
                 def _():
                     start_hop(
-                        way, src, send_sem.at[r, m, i], m, i, real(way, z), real(way, z),
+                        way, src, send_sem.at[r], m, i, real(way, z), real(way, z),
                         real(way, j),
                     )
             return 0
@@ -873,17 +931,17 @@
     elsewhere(forward)
     for n in range(len(sends), len(units)):
         do_unit(n)
-    for other in range(1, tps):
-        for s in range(count):
-            spread(s, lax.rem(t + other, tps)).wait_recv()
+    spread().wait_recv()
     normalise()
     gate_up(z, True)
 
-    def take_piece(way, m, item, i):
+    def take_piece(way, m, item, i, ready, wide=None):
         k = real(way, z)
         l, at = cut(i)
 
-        @pl.when(item < k * (count - k))
+        mine = True if wide is None else (2 * k >= count) == wide
+
+        @pl.when((item < k * (count - k)) & mine)
         def _():
             s = k - 1 - item // (count - k)
             dd = count - 1 - lax.rem(item, count - k)
@@ -891,33 +949,36 @@
 
             def awaited(ref):
                 remote(
-                    ref, ref, send_sem.at[0, m, i], recv_sem.at[way, item, m, i], "fs", source
+                    ref, ref, send_sem.at[0], recv_sem.at[way, item, m, i], "fs", source
                 ).wait_recv()
 
             @pl.when(dd == k)
             def _():
                 awaited(spot(m, l, at, source, y))
-                for other in range(1, groups):
-                    passing(source, m, i, other).start()
+                ready(source, m, i)
 
             @pl.when(dd > k)
             def _():
                 slot = (k - 1 - s) * (count - 1 - k) + (count - 1 - dd)
                 ref = transit.at[way, slot, m, l, pl.ds(at, piece), :]
                 awaited(ref)
-                start_hop(way, ref, relay_sem.at[way, slot, m, i], m, i, k, s, dd)
-
-    def settled(way, item, body):
+                start_hop(way, ref, relay_sem.at[way, slot], m, i, k, s, dd)
+
+    def settled(way, item, body, wide=None):
         k = real(way, z)
         kept = jnp.maximum(item, 0)
         s = k - 1 - kept // (count - k)
         dd = count - 1 - lax.rem(kept, count - k)
 
-        @pl.when((item >= 0) & (item < k * (count - k)) & (dd == k))
+        mine = True if wide is None else (2 * k >= count) == wide
+
+        @pl.when((item >= 0) & (item < k * (count - k)) & (dd == k) & mine)
         def _():
             body(real(way, s))
 
-    most = max(k * (count - k) for k in range(count))
+    def pass_on(source, m, i):
+        for other in range(1, groups):
+            passing(source, m, i, other).start()
 
     def await_pass(s, m, i):
         for other in range(1, groups):
@@ -936,7 +997,7 @@
         for m in (0, 1):
             def one(i, _):
                 for way in (0, 1):
-                    take_piece(way, m, n, i)
+                    take_piece(way, m, n, i, pass_on)
                 return 0
 
             lax.fori_loop(0, pieces, one, 0)
@@ -952,88 +1013,148 @@
 
     lax.fori_loop(0, most + 1, early, 0)
     activate()
+    def at_middle(body):
+        @pl.when((z * (count - z) == most) | ((count - 1 - z) * (z + 1) == most))
+        def _():
+            for other in range(1, groups):
+                body(other)
+
+    at_middle(lambda other: lending(other).start())
 
     def own_down(i, _):
-        down_piece(z, i)
+        down_piece(z, i, range(groups))
         return 0
 
     lax.fori_loop(0, pieces, own_down, 0)
-
-    lag, wait_for = 2, 4
-
-    def later(p, _):
-        n, i = p // pieces, lax.rem(p, pieces)
-        for way in (0, 1):
-            take_piece(way, 2, n, i)
-        q = p - lag
-        before = jnp.maximum(q, 0)
-
-        def work(s):
-            j = lax.rem(before, pieces)
-            await_pass(s, 2, j)
-            down_piece(s, j)
-
-        for way in (0, 1):
-            settled(way, jnp.where(q >= 0, before // pieces, -1), work)
-
-        @pl.when((p == 1) & (z == t))
-        def _():
-            give_back()
-
-        q = p - wait_for
-        done = jnp.maximum(q, 0)
-
-        def close(s):
-            @pl.when((s == t) & (lax.rem(done, pieces) == pieces - 1))
-            def _():
-                give_back()
-
-        for way in (0, 1):
-            settled(way, jnp.where(q >= 0, done // pieces, -1), close)
-        return 0
-
-    lax.fori_loop(0, most * pieces + wait_for, later, 0)
 
     def sent(ref, sem):
         remote(ref, ref, sem, recv_sem.at[0, 0, 0, 0], "grp", lax.rem(y + 1, groups)).wait_send()
 
-    def drain(i, _):
-        l, at = cut(i)
-        for m in range(3):
-            for r in range(count - 1):
-                sent(stage.at[r, m, l, pl.ds(at, piece), :], send_sem.at[r, m, i])
-
-                def passed(s):
-                    for other in range(1, groups):
-                        passing(s, m, i, other).wait_send()
-
-                passed(ranked(r))
-            for slot in range(transit.shape[1]):
+    def drain():
+        for r in range(count - 1):
+            sent(stage.at[r], send_sem.at[r])
+            for m in range(3):
+                base = pl.multiple_of(ranked(r) * rows + y * share, share)
+                for other in range(1, groups):
+                    sent(
+                        landing[m].at[:, pl.ds(base, share), :],
+                        pass_send.at[ranked(r), m, other - 1],
+                    )
+        for slot in range(transit.shape[1]):
+            @pl.when(slot < z * (count - 1 - z))
+            def _():
                 for way in (0, 1):
-                    @pl.when(slot < z * (count - 1 - z))
-                    def _():
-                        sent(
-                            transit.at[way, slot, m, l, pl.ds(at, piece), :],
-                            relay_sem.at[way, slot, m, i],
-                        )
+                    sent(transit.at[way, slot], relay_sem.at[way, slot])
+
+    def own_close(i, _):
+        close_piece(i)
+        return 0
+
+    def whole(p):
+        return p // pieces, lax.rem(p, pieces)
+
+    def work(s, i):
+        await_pass(s, 2, i)
+        down_piece(s, i, range(groups))
+
+    def later(wide, span):
+        def one(p, _):
+            n, i = whole(p)
+
+            @pl.when(p < span)
+            def _():
+                for way in (0, 1):
+                    take_piece(way, 2, n, i, pass_on, wide)
+
+            def trail(lag, body):
+                n, i = whole(jnp.maximum(p - lag, 0))
+                due = (p >= lag) & (p < span + lag)
+                for way in (0, 1):
+                    settled(way, jnp.where(due, n, -1), lambda s: body(s, i), wide)
+
+            def close(s, i):
+                @pl.when(s == t)
+                def _():
+                    close_piece(i)
+
+            trail(1, work)
+            trail(3, close)
+            return 0
+
+        lax.fori_loop(0, span + 3, one, 0)
+
+    def ending(i, _):
+        for way in (0, 1):
+            take_piece(way, 2, most - 1, i, pass_on)
+        for way in (0, 1):
+            settled(way, jnp.where(i >= 1, most - 1, -1), lambda s: work(s, jnp.maximum(i - 1, 0)))
+        return 0
+
+    narrow = max([k * (count - k) for k in range(count) if 2 * k < count])
+    later(False, narrow * pieces)
+    at_middle(lambda other: lent(other).wait_recv())
+
+    @pl.when(z == t)
+    def _():
+        lax.fori_loop(0, pieces, own_close, 0)
+
+    later(True, (most - 1) * pieces)
+    lax.fori_loop(0, final, ending, 0)
+    for way in (0, 1):
+        def use(source, m, i, way=way):
+            down_last(way, source)
+            pass_on(source, m, i)
+
+        take_piece(way, 2, most - 1, final, use)
+    for way in (0, 1):
+        settled(way, most - 1, lambda s: work(s, final - 1))
+
+    inner = jnp.where(z < half, z + 1 < half, z - 1 >= half)
+    outer = jnp.where(z < half, z - 1, z + 1)
+
+    @pl.when(inner)
+    def _():
+        pl.semaphore_wait(go_sem, 1)
+
+    @pl.when((outer >= 0) & (outer < count))
+    def _():
+        pl.semaphore_signal(go_sem, inc=1, device_id={"fs": outer}, device_id_type=MESH)
+
+    @pl.when(last)
+    def _():
+        lax.fori_loop(0, pieces, own_close, 0)
+
+    give_back()
+    drain()
+
+    def drain_more(i, _):
         for s in range(count):
-            @pl.when(s != t)
+            for giver in range(groups):
+                skipped = comes_last(s) & (y != giver) & (i == final)
+
+                @pl.when((s != t) & jnp.logical_not(skipped))
+                def _():
+                    part_copy(s, i, giver).wait_send()
+        for way in (0, 1):
+            k = real(way, z)
+
+            @pl.when((k * (count - k) == most) & (i == final))
             def _():
-                for giver in range(groups):
-                    part_copy(s, i, giver).wait_send()
+                await_pass(real(way, 0), 2, i)
+                for other in range(1, groups):
+                    part_across(way, real(way, 0), other).wait_send()
         return 0
 
-    lax.fori_loop(0, pieces, drain, 0)
+    lax.fori_loop(0, pieces, drain_more, 0)
+    at_middle(lambda other: lending(other).wait_send())
     elsewhere(lambda j: dispatching(j).wait_send())
-    for other in range(1, tps):
-        for s in range(count):
-            spreading(s, other).wait_send()
+    spread().wait_send()
 
     elsewhere(lambda s: returned(s).wait_recv())
     back = land_ret[...].reshape(experts * capacity, columns)
-    over = (((0,), (0,)), ((), ()))
-    value = lax.dot_general(combine_w[0], back, over, preferred_element_type=f32)
-    value = value + lax.dot_general(combine_w[1], back, over, preferred_element_type=f32)
+    used = experts * capacity
+    value = jnp.dot(combine_w[0, :, :used], back, preferred_element_type=f32)
+    value = value + jnp.dot(combine_w[1, :, :used], back, preferred_element_type=f32)
     mixed_o[...] = value.astype(bf16)
     elsewhere(lambda j: returning(j).wait_send())
 
@@ -1061,7 +1182,7 @@
     local, own_tokens, columns = experts // count, *tokens.shape
     capacity = own_tokens * 5 // 16
     share = rows // groups
-    parts = max(1, share // 128)
+    parts = share // 128
     pieces = local * parts
     tall = count * capacity
     dims = (groups, count, tps, local, rows, width, parts, experts, capacity)
@@ -1087,17 +1208,19 @@
             pltpu.VMEM((tps, count) + block, bf16),
             pltpu.VMEM((local, tall, tps * columns), bf16),
             pltpu.VMEM((2, local, tall, width), f32),
-            pltpu.VMEM((local, tall, width), bf16),
+            pltpu.VMEM((groups, local, tall, width), bf16),
             pltpu.VMEM((count, local, tall, columns), bf16),
+            pltpu.VMEM((2, groups - 1, tall, 128), bf16),
             pltpu.VMEM((tps, local, tall, columns), bf16),
-            pltpu.VMEM((2, experts * capacity, own_tokens), bf16),
+            pltpu.VMEM((2, own_tokens, -(-experts * capacity // 128) * 128), bf16),
             pltpu.VMEM((count,) + block, bf16),
             pltpu.VMEM((count,) + block, bf16),
-            sem((3,)), sem((count - 1, 3, pieces)), sem((2, items, 3, pieces)),
-            sem((2, slots, 3, pieces)),
-            sem((count, 3, pieces, groups - 1)), sem((count, 3, pieces, groups - 1)),
-            sem((count,)), sem((count,)), sem((tps, count)), sem((tps, count)),
+            sem((3,)), sem((count - 1,)), sem((2, items, 3, pieces)), sem((2, slots)),
+            sem((count, 3, groups - 1)), sem((count, 3, pieces, groups - 1)),
+            sem((count,)), sem((count,)), sem((1,)), sem((1,)),
             sem((count, pieces, groups)), sem((tps, pieces, groups)), sem((count,)), sem((count,)),
+            sem((2, groups - 1)), sem((groups,)), sem((groups,)),
+            pltpu.SemaphoreType.REGULAR,
         ],
         compiler_params=pltpu.CompilerParams(
             collective_id=1, has_side_effects=True, vmem_limit_bytes=38 * 1024 * 1024

time: 316 us -> 309 us (0.978)
  Pallas kernels: 315 us -> 309 us
    pallas_call x1, Pallas kernels: 306 us -> 300 us  [fused(): pl.pallas_call(functools.partial(fused_kernel, dims), out_shape=[pltpu.VM...]
where the time goes in v2:
time: 309 us
  Pallas kernels  309 us (100%)
    pallas_call x1, Pallas kernels, fused(): pl.pallas_call(functools.partial(fused_kernel, dims), out_shape=[pltpu.VM...  300 us
    pallas_call x1, Pallas kernels, fused(): pl.pallas_call(functools.partial(writer_kernel, parts), out_shape=[jax.Sh...  8.63 us

profile of v2, /device:TPU:0, one launch (start us, length us, event | category | flops | bytes accessed | tf_op | source)
XLA Modules:
  0.0 309.2 jit_solution(3313216035401317864)
XLA Ops:
  0.6 299.9 %shard_map.102 = (bf16[2,2048,1024]{2,1,0:T(8,128)(2,1)S(1)}, bf16[2,2048,1024]{2,1,0:T(8,128)(2,1)S(1)}, bf16[2,2048,1024]{2,1,0:T(8,128)(2,1)S(1)}, bf16[128,5...) custom-call(bf16[128,512]{1,0:T(8,128)(2,1)} %tokens.1, s32[2,128]{1,0:T(2,128)} %bitcast.4, f32[2,128]{1,0:T(2,128)} %bitcast.5, ...), custom_call_target="tpu_custom_call" | custom-call | tf_op jit(solution)/shard_map/pallas_call | solution.py:1195
  300.6 8.6 %shard_map.103 = (bf16[2,2048,1024]{2,1,0:T(8,128)(2,1)}, bf16[2,2048,1024]{2,1,0:T(8,128)(2,1)}, bf16[2,2048,1024]{2,1,0:T(8,128)(2,1)}, bf16[128,512]{1,0:T(8,128)(2,1)}) custom-call(bf16[2,2048,1024]{2,1,0:T(8,128)(2,1)S(1)} %get-tuple-element.8.refs_0_, bf16[2,2048,1024]{2,1,0:T(8,128)(2,1)S(1)} %get-tuple-element.9.refs_1_, ...), custom_call_target="tpu_custom_call" | custom-call | tf_op jit(solution)/shard_map/pallas_call | solution.py:1233

commit v3 on v2

--- a/solution.py
+++ b/solution.py
@@ -536,15 +536,21 @@
     return table
 
 
-def fused_kernel(
-    dims, tokens, routes, route_weights, gains, gate_w, up_w, down_w,
-    gate_o, up_o, down_o, mixed_o, transit,
-    raw, stage, gain_col, scales, send_x, land_x, normed, sums, hidden, partial, across, summing, combine_w,
-    send_ret, land_ret,
-    load_sem, send_sem, recv_sem, relay_sem, pass_send, pass_recv,
-    x_send, x_recv, xg_send, xg_recv, part_send, part_recv, ret_send, ret_recv,
-    across_send, hid_send, hid_recv, go_sem,
-):
+def mates(count):
+    paired = count & (count - 1) == 0
+    return [[k ^ d if paired else (k + d) % count for k in range(count)] for d in range(count)]
+
+
+def fused_kernel(dims, *refs):
+    count = dims[1]
+    (tokens, routes, route_weights, gains, gate_w, up_w, down_w), refs = refs[:7], refs[7:]
+    (gate_o, up_o, down_o, transit, combine_w), refs = refs[:5], refs[5:]
+    back_o, refs = refs[:count], refs[count:]
+    (
+        raw, stage, gain_col, scales, send_x, land_x, normed, sums, hidden, partial, across, summing,
+        load_sem, send_sem, recv_sem, relay_sem, pass_send, pass_recv,
+        x_send, x_recv, xg_send, xg_recv, part_send, part_recv, across_send, hid_send, hid_recv,
+    ) = refs
     groups, count, tps, local, rows, width, parts, experts, capacity = dims
     weights, landing = (gate_w, up_w, down_w), (gate_o, up_o, down_o)
     y, z, t = lax.axis_index("grp"), lax.axis_index("fs"), lax.axis_index("tp")
@@ -652,21 +658,33 @@
 
     def pack():
         found = slot_rows()
-        shape = (combine_w.shape[2], own_tokens)
+        shape = (experts * capacity, own_tokens)
         slot_ids = lax.broadcasted_iota(jnp.int32, shape, 0)
-        chosen, weighed = jnp.zeros(shape, f32), jnp.zeros(shape, f32)
-        for k, slot in enumerate(found):
-            hit = slot_ids == slot
-            chosen = jnp.where(hit, 1.0, chosen)
-            weighed = weighed + jnp.where(hit, route_weights[k : k + 1, :], 0.0)
+        chosen = jnp.zeros(shape, f32)
+        for slot in found:
+            chosen = jnp.where(slot_ids == slot, 1.0, chosen)
         packed = jnp.dot(chosen.astype(bf16), tokens[...], preferred_element_type=f32)
         packed = packed.astype(bf16)
         for j in range(count):
             send_x[j] = packed[j * block_rows : (j + 1) * block_rows, :]
-        weighed = jnp.transpose(weighed)
-        high = weighed.astype(bf16)
-        combine_w[0] = high
-        combine_w[1] = (weighed - high.astype(f32)).astype(bf16)
+
+    def weigh():
+        found = slot_rows()
+        shape = (combine_w.shape[3], own_tokens)
+        places = lax.broadcasted_iota(jnp.int32, shape, 0)
+        for d in range(count):
+            source = sum(
+                (z == k).astype(jnp.int32) * mates(count)[d].index(k) for k in range(count)
+            )
+            first = source * block_rows
+            weighed = jnp.zeros(shape, f32)
+            for k, slot in enumerate(found):
+                hit = (places + first == slot) & (places < block_rows)
+                weighed = weighed + jnp.where(hit, route_weights[k : k + 1, :], 0.0)
+            weighed = jnp.transpose(weighed)
+            high = weighed.astype(bf16)
+            combine_w[d, 0] = high
+            combine_w[d, 1] = (weighed - high.astype(f32)).astype(bf16)
 
     def dispatching(j):
         return remote(send_x.at[j], land_x.at[t, z], x_send.at[j], x_recv.at[z], "fs", j)
@@ -736,7 +754,6 @@
 
         lax.fori_loop(0, local * (width // tile), one, 0)
 
-    half = count // 2
     most = max(k * (count - k) for k in range(count))
 
     def comes_last(s):
@@ -835,31 +852,13 @@
                 value = value + summing[peer, l, :, col].astype(f32)
             sums[0, l, :, col] = value
 
-    def returning(j):
-        return remote(send_ret.at[j], land_ret.at[z], ret_send.at[j], ret_recv.at[z], "fs", j)
-
-    def returned(s):
-        return remote(send_ret.at[s], land_ret.at[s], ret_send.at[s], ret_recv.at[s], "fs", s)
-
     def give_back():
-        for j in range(count):
-            block = jnp.concatenate(
-                [
-                    sums[0, l, j * capacity : (j + 1) * capacity, :columns]
-                    for l in range(local)
-                ],
-                axis=0,
+        for d in range(count):
+            target = sum((z == k).astype(jnp.int32) * mates(count)[d][k] for k in range(count))
+            first = pl.multiple_of(target * capacity, 8)
+            back_o[d][...] = jnp.concatenate(
+                [sums[0, l, pl.ds(first, capacity), :columns] for l in range(local)], axis=0
             ).astype(bf16)
-
-            @pl.when(z == j)
-            def _():
-                land_ret[j] = block
-
-            @pl.when(z != j)
-            def _():
-                send_ret[j] = block
-        for r in range(count - 1):
-            returning(ranked(r)).start()
 
     sends = [(r, m, None) for r in range(count - 1) for m in (0, 1)]
     keeps = [(None, m, g) for m in (0, 1) for g in range(groups)]
@@ -932,6 +931,7 @@
     for n in range(len(sends), len(units)):
         do_unit(n)
     spread().wait_recv()
+    weigh()
     normalise()
     gate_up(z, True)
 
@@ -1109,17 +1109,6 @@
     for way in (0, 1):
         settled(way, most - 1, lambda s: work(s, final - 1))
 
-    inner = jnp.where(z < half, z + 1 < half, z - 1 >= half)
-    outer = jnp.where(z < half, z - 1, z + 1)
-
-    @pl.when(inner)
-    def _():
-        pl.semaphore_wait(go_sem, 1)
-
-    @pl.when((outer >= 0) & (outer < count))
-    def _():
-        pl.semaphore_signal(go_sem, inc=1, device_id={"fs": outer}, device_id_type=MESH)
-
     @pl.when(last)
     def _():
         lax.fori_loop(0, pieces, own_close, 0)
@@ -1150,17 +1139,9 @@
     elsewhere(lambda j: dispatching(j).wait_send())
     spread().wait_send()
 
-    elsewhere(lambda s: returned(s).wait_recv())
-    back = land_ret[...].reshape(experts * capacity, columns)
-    used = experts * capacity
-    value = jnp.dot(combine_w[0, :, :used], back, preferred_element_type=f32)
-    value = value + jnp.dot(combine_w[1, :, :used], back, preferred_element_type=f32)
-    mixed_o[...] = value.astype(bf16)
-    elsewhere(lambda j: returning(j).wait_send())
-
 
 def writer_kernel(parts, *refs):
-    ins, outs, sem = refs[:4], refs[4:8], refs[8]
+    ins, outs, sem = refs[:3], refs[3:6], refs[6]
     local, high = ins[0].shape[:2]
     step = high // parts
 
@@ -1168,12 +1149,23 @@
         at = pl.ds(i * step, step)
         return pltpu.make_async_copy(ins[k].at[l, at, :], outs[k].at[l, at, :], sem.at[k, l, i])
 
-    small = pltpu.make_async_copy(ins[3], outs[3], sem.at[3, 0, 0])
-    jobs = [copy(k, l, i) for k in range(3) for l in range(local) for i in range(parts)] + [small]
+    jobs = [copy(k, l, i) for k in range(3) for l in range(local) for i in range(parts)]
     for job in jobs:
         job.start()
     for job in jobs:
         job.wait()
+
+
+def combine_kernel(weights, *refs):
+    value = None
+    for d, back in enumerate(refs[:-1]):
+        for part in range(2):
+            term = jnp.dot(
+                weights[d, part, :, : back.shape[0]], back[...],
+                preferred_element_type=jnp.float32,
+            )
+            value = term if value is None else value + term
+    refs[-1][...] = value.astype(refs[-1].dtype)
 
 
 def fused(tokens, routes, route_weights, norm_gain, gate_weight, up_weight, down_weight):
@@ -1192,13 +1184,15 @@
     bf16, f32, sem = jnp.bfloat16, jnp.float32, pltpu.SemaphoreType.DMA
     vmem, anywhere = pl.BlockSpec(memory_space=pltpu.VMEM), pl.BlockSpec(memory_space=pl.ANY)
     block = (local * capacity, columns)
-    gate, up, down, mixed, _ = pl.pallas_call(
+    lanes = -(-block[0] // 128) * 128
+    gate, up, down, _, weights, *backs = pl.pallas_call(
         functools.partial(fused_kernel, dims),
         out_shape=[pltpu.VMEM(shape, bf16)] * 3
-        + [pltpu.VMEM(tokens.shape, bf16)]
-        + [jax.ShapeDtypeStruct((2, slots, 3, local, share, width), bf16)],
+        + [jax.ShapeDtypeStruct((2, slots, 3, local, share, width), bf16)]
+        + [jax.ShapeDtypeStruct((count, 2, own_tokens, lanes), bf16)]
+        + [jax.ShapeDtypeStruct(block, bf16)] * count,
         in_specs=[vmem] * 4 + [anywhere] * 3,
-        out_specs=[vmem] * 4 + [anywhere],
+        out_specs=[vmem] * 3 + [anywhere] + [vmem] * (1 + count),
         scratch_shapes=[
             pltpu.VMEM((3, local, share, width), f32),
             pltpu.VMEM((count - 1, 3, local, share, width), bf16),
@@ -1212,15 +1206,11 @@
             pltpu.VMEM((count, local, tall, columns), bf16),
             pltpu.VMEM((2, groups - 1, tall, 128), bf16),
             pltpu.VMEM((tps, local, tall, columns), bf16),
-            pltpu.VMEM((2, own_tokens, -(-experts * capacity // 128) * 128), bf16),
-            pltpu.VMEM((count,) + block, bf16),
-            pltpu.VMEM((count,) + block, bf16),
             sem((3,)), sem((count - 1,)), sem((2, items, 3, pieces)), sem((2, slots)),
             sem((count, 3, groups - 1)), sem((count, 3, pieces, groups - 1)),
             sem((count,)), sem((count,)), sem((1,)), sem((1,)),
-            sem((count, pieces, groups)), sem((tps, pieces, groups)), sem((count,)), sem((count,)),
+            sem((count, pieces, groups)), sem((tps, pieces, groups)),
             sem((2, groups - 1)), sem((groups,)), sem((groups,)),
-            pltpu.SemaphoreType.REGULAR,
         ],
         compiler_params=pltpu.CompilerParams(
             collective_id=1, has_side_effects=True, vmem_limit_bytes=38 * 1024 * 1024
@@ -1229,16 +1219,30 @@
         tokens, routes.T, route_weights.T, norm_gain.reshape(rows // 128, 128),
         gate_weight, up_weight, down_weight,
     )
+    arrived = [backs[0]] + [
+        lax.ppermute(backs[d], "fs", list(enumerate(mates(count)[d])))
+        for d in range(1, count)
+    ]
     parts = max(1, shape[1] // 512)
-    return pl.pallas_call(
+    outs = pl.pallas_call(
         functools.partial(writer_kernel, parts),
-        out_shape=[jax.ShapeDtypeStruct(shape, bf16)] * 3
-        + [jax.ShapeDtypeStruct(tokens.shape, bf16)],
-        in_specs=[vmem] * 4,
-        out_specs=[anywhere] * 4,
-        scratch_shapes=[sem((4, local, parts))],
+        out_shape=[jax.ShapeDtypeStruct(shape, bf16)] * 3,
+        in_specs=[vmem] * 3,
+        out_specs=[anywhere] * 3,
+        scratch_shapes=[sem((3, local, parts))],
         compiler_params=pltpu.CompilerParams(vmem_limit_bytes=1024 * 1024),
-    )(gate, up, down, mixed)
+        cost_estimate=pl.CostEstimate(
+            flops=10**11, bytes_accessed=12 * local * count * rows * width, transcendentals=0
+        ),
+    )(gate, up, down)
+    mixed = pl.pallas_call(
+        combine_kernel,
+        out_shape=jax.ShapeDtypeStruct(tokens.shape, bf16),
+        in_specs=[vmem] * (1 + count),
+        out_specs=vmem,
+        compiler_params=pltpu.CompilerParams(vmem_limit_bytes=8 * 1024 * 1024),
+    )(weights, *arrived)
+    return *outs, mixed
 
 
 def on_device(tokens, routes, route_weights, norm_gain, gate_weight, up_weight, down_weight):

time: 309 us -> 309 us (level)
  Pallas kernels: 309 us -> 302 us
  starting transfers between devices: 0 us -> 6.5 us
    pallas_call x1, Pallas kernels: 300 us -> 292 us  [fused(): pl.pallas_call(functools.partial(fused_kernel, dims), out_shape=[pltpu.VM...]
    ppermute x0 -> x3, starting transfers between devices: none -> 6.5 us  [fused(): lax.ppermute(backs[d], 'fs', list(enumerate(mates(count)[d])))]
  transfers between devices with their start and end apart: 0 -> 3, of which waited for: 0 -> 0; matrix products, arithmetic and copies ran while one was open for 0% -> 0% of each run, Pallas kernels for 0% -> 3%
where the time goes in v3:
time: 309 us
  Pallas kernels  302 us (98%)
  starting transfers between devices  6.5 us (2%)
    pallas_call x1, Pallas kernels, fused(): pl.pallas_call(functools.partial(fused_kernel, dims), out_shape=[pltpu.VM...  292 us
    pallas_call x1, Pallas kernels, fused(): pl.pallas_call(functools.partial(writer_kernel, parts), out_shape=[jax.Sh...  8.55 us
    ppermute x3, starting transfers between devices, fused(): lax.ppermute(backs[d], 'fs', list(enumerate(mates(count)[d])))  6.5 us
  transfers between devices with their start and end apart: 3, of which 0 were waited for; matrix products, arithmetic and copies ran while one was open for 0% of the time, Pallas kernels for 3%

profile of v3, /device:TPU:0, one launch (start us, length us, event | category | flops | bytes accessed | tf_op | source)
XLA Modules:
  0.0 309.2 jit_solution(15601326999407331090)
XLA Ops:
  0.6 292.3 %shard_map.102 = (bf16[2,2048,1024]{2,1,0:T(8,128)(2,1)S(1)}, bf16[2,2048,1024]{2,1,0:T(8,128)(2,1)S(1)}, bf16[2,2048,1024]{2,1,0:T(8,128)(2,1)S(1)}, bf16[2,2,3...) custom-call(bf16[128,512]{1,0:T(8,128)(2,1)} %refs_0_.1, ...), custom_call_target="tpu_custom_call" | custom-call | tf_op jit(solution)/shard_map/pallas_call | solution.py:1188
  293.0 3.3 %collective-permute-start = (bf16[80,512]{1,0:T(8,128)(2,1)}, bf16[80,512]{1,0:T(8,128)(2,1)S(1)}, u32[]{:S(2)}, u32[]{:S(2)}) collective-permute-start(bf16[80,512]{1,0:T(8,128)(2,1)} %get-tuple-element.23), channel_id=1, source_target_pairs={{0,4},{4,0},{8,12},{12,8},{1,5},{5,1},{9,13},{13,9},{2,6},{6,2},{1... | collective-permute-start | bytes 245768 | tf_op jit(solution)/shard_map/ppermute | solution.py:1223
  296.3 3.1 %collective-permute-start.1 = (bf16[80,512]{1,0:T(8,128)(2,1)}, bf16[80,512]{1,0:T(8,128)(2,1)S(1)}, u32[]{:S(2)}, u32[]{:S(2)}) collective-permute-start(bf16[80,512]{1,0:T(8,128)(2,1)} %get-tuple-element.24), channel_id=1, source_target_pairs={{0,8},{4,12},{8,0},{12,4},{1,9},{5,13},{9,1},{13,5},{2,10},{6,14},... | collective-permute-start | bytes 245768 | tf_op jit(solution)/shard_map/ppermute | solution.py:1223
  299.5 0.0 collective-permute-start.2
  299.5 0.0 copy-start
  299.5 0.0 copy-start.1
  299.5 8.6 %shard_map.103 = (bf16[2,2048,1024]{2,1,0:T(8,128)(2,1)}, bf16[2,2048,1024]{2,1,0:T(8,128)(2,1)}, bf16[2,2048,1024]{2,1,0:T(8,128)(2,1)}) custom-call(bf16[2,2048,1024]{2,1,0:T(8,128)(2,1)S(1)} %get-tuple-element.15.refs_0_, bf16[2,2048,1024]{2,1,0:T(8,128)(2,1)S(1)} %get-tuple-element.16.refs_1_, bf16[2,2048,1024]{2,1,0:T(8,128)(2,1)S(1)} %get-tuple-element.17.refs_2_), custom_call_target="tpu_custom_call" | custom-call | flops 99999997952 | bytes 50331648 | tf_op jit(solution)/shard_map/pallas_call | solution.py:1227
  308.0 0.0 collective-permute-done.refs_1_
  308.0 0.0 collective-permute-done.1.refs_2_
  308.1 0.0 collective-permute-done.2.refs_3_
  308.1 0.0 copy-done
  308.1 0.0 copy-done.1
  308.1 1.1 shard_map.104
Async XLA Ops:
  293.0 15.1 %collective-permute-start = (bf16[80,512]{1,0:T(8,128)(2,1)}, bf16[80,512]{1,0:T(8,128)(2,1)S(1)}, u32[]{:S(2)}, u32[]{:S(2)}) collective-permute-start(bf16[80,512]{1,0:T(8,128)(2,1)} %get-tuple-element.23), channel_id=1, source_target_pairs={{0,4},{4,0},{8,12},{12,8},{1,5},{5,1},{9,13},{13,9},{2,6},{6,2},{1... | collective-permute-start | bytes 245768 | tf_op jit(solution)/shard_map/ppermute | solution.py:1223
  296.3 11.7 %collective-permute-start.1 = (bf16[80,512]{1,0:T(8,128)(2,1)}, bf16[80,512]{1,0:T(8,128)(2,1)S(1)}, u32[]{:S(2)}, u32[]{:S(2)}) collective-permute-start(bf16[80,512]{1,0:T(8,128)(2,1)} %get-tuple-element.24), channel_id=1, source_target_pairs={{0,8},{4,12},{8,0},{12,4},{1,9},{5,13},{9,1},{13,5},{2,10},{6,14},... | collective-permute-start | bytes 245768 | tf_op jit(solution)/shard_map/ppermute | solution.py:1223
  299.5 8.6 %collective-permute-start.2 = (bf16[80,512]{1,0:T(8,128)(2,1)}, bf16[80,512]{1,0:T(8,128)(2,1)S(1)}, u32[]{:S(2)}, u32[]{:S(2)}) collective-permute-start(bf16[80,512]{1,0:T(8,128)(2,1)} %get-tuple-element.25), channel_id=1, source_target_pairs={{0,12},{4,8},{8,4},{12,0},{1,13},{5,9},{9,5},{13,1},{2,14},{6,10},... | collective-permute-start | bytes 245768 | tf_op jit(solution)/shard_map/ppermute | solution.py:1223
  299.5 8.6 %copy-start = (bf16[4,2,128,128]{3,2,1,0:T(8,128)(2,1)S(1)}, bf16[4,2,128,128]{3,2,1,0:T(8,128)(2,1)}, u32[]{:S(2)}) copy-start(bf16[4,2,128,128]{3,2,1,0:T(8,128)(2,1)} %get-tuple-element.21.weights) | copy-start | bytes 786436
  299.5 8.6 %copy-start.1 = (bf16[80,512]{1,0:T(8,128)(2,1)S(1)}, bf16[80,512]{1,0:T(8,128)(2,1)}, u32[]{:S(2)}) copy-start(bf16[80,512]{1,0:T(8,128)(2,1)} %get-tuple-element.22.refs_0_) | copy-start | bytes 245764

commit v4 on v2

--- a/solution.py
+++ b/solution.py
@@ -543,7 +543,7 @@
     send_ret, land_ret,
     load_sem, send_sem, recv_sem, relay_sem, pass_send, pass_recv,
     x_send, x_recv, xg_send, xg_recv, part_send, part_recv, ret_send, ret_recv,
-    across_send, hid_send, hid_recv, go_sem,
+    across_send, hid_send, hid_recv,
 ):
     groups, count, tps, local, rows, width, parts, experts, capacity = dims
     weights, landing = (gate_w, up_w, down_w), (gate_o, up_o, down_o)
@@ -736,7 +736,6 @@
 
         lax.fori_loop(0, local * (width // tile), one, 0)
 
-    half = count // 2
     most = max(k * (count - k) for k in range(count))
 
     def comes_last(s):
@@ -1108,17 +1107,6 @@
         take_piece(way, 2, most - 1, final, use)
     for way in (0, 1):
         settled(way, most - 1, lambda s: work(s, final - 1))
-
-    inner = jnp.where(z < half, z + 1 < half, z - 1 >= half)
-    outer = jnp.where(z < half, z - 1, z + 1)
-
-    @pl.when(inner)
-    def _():
-        pl.semaphore_wait(go_sem, 1)
-
-    @pl.when((outer >= 0) & (outer < count))
-    def _():
-        pl.semaphore_signal(go_sem, inc=1, device_id={"fs": outer}, device_id_type=MESH)
 
     @pl.when(last)
     def _():
@@ -1220,7 +1208,6 @@
             sem((count,)), sem((count,)), sem((1,)), sem((1,)),
             sem((count, pieces, groups)), sem((tps, pieces, groups)), sem((count,)), sem((count,)),
             sem((2, groups - 1)), sem((groups,)), sem((groups,)),
-            pltpu.SemaphoreType.REGULAR,
         ],
         compiler_params=pltpu.CompilerParams(
             collective_id=1, has_side_effects=True, vmem_limit_bytes=38 * 1024 * 1024

time: 309 us -> 309 us (level)
  no operation moved by 1% of the time
where the time goes in v4:
time: 309 us
  Pallas kernels  309 us (100%)
    pallas_call x1, Pallas kernels, fused(): pl.pallas_call(functools.partial(fused_kernel, dims), out_shape=[pltpu.VM...  300 us
    pallas_call x1, Pallas kernels, fused(): pl.pallas_call(functools.partial(writer_kernel, parts), out_shape=[jax.Sh...  8.63 us

profile of v4, /device:TPU:0, one launch (start us, length us, event | category | flops | bytes accessed | tf_op | source)
XLA Modules:
  0.0 309.2 jit_solution(13348566177346945243)
XLA Ops:
  0.6 299.9 %shard_map.102 = (bf16[2,2048,1024]{2,1,0:T(8,128)(2,1)S(1)}, bf16[2,2048,1024]{2,1,0:T(8,128)(2,1)S(1)}, bf16[2,2048,1024]{2,1,0:T(8,128)(2,1)S(1)}, bf16[128,5...) custom-call(bf16[128,512]{1,0:T(8,128)(2,1)} %tokens.1, s32[2,128]{1,0:T(2,128)} %bitcast.4, f32[2,128]{1,0:T(2,128)} %bitcast.5, ...), custom_call_target="tpu_custom_call" | custom-call | tf_op jit(solution)/shard_map/pallas_call | solution.py:1183
  300.5 8.6 %shard_map.103 = (bf16[2,2048,1024]{2,1,0:T(8,128)(2,1)}, bf16[2,2048,1024]{2,1,0:T(8,128)(2,1)}, bf16[2,2048,1024]{2,1,0:T(8,128)(2,1)}, bf16[128,512]{1,0:T(8,128)(2,1)}) custom-call(bf16[2,2048,1024]{2,1,0:T(8,128)(2,1)S(1)} %get-tuple-element.8.refs_0_, bf16[2,2048,1024]{2,1,0:T(8,128)(2,1)S(1)} %get-tuple-element.9.refs_1_, ...), custom_call_target="tpu_custom_call" | custom-call | tf_op jit(solution)/shard_map/pallas_call | solution.py:1220
